TPU v7x, 128 devices: a whole 4x4x4 slice. The times are simulated.
128 devices in a mesh: fs: 16 (over z, y), tp: 8 (over x, core).
Axes of the slice: x: 4, y: 4, z: 4, core: 2. Of those that a mesh axis runs over, the one named last changes fastest.
Arguments:
- mixed: bfloat16 [49152, 2048], P(('fs', 'tp')), may hold values from -6 to 6
- residual: bfloat16 [49152, 2048], P(('fs', 'tp')), may hold values from -6 to 6
- mix_weight: bfloat16 [2048, 2048], P(('fs', 'tp')), may hold values from -0.125 to 0.125
- norm_gain: float32 [2048], replicated, may hold values from 0.1 to 1.9
- up_weight: bfloat16 [2048, 5504], P('fs', 'tp'), may hold values from -0.125 to 0.125
- gate_weight: bfloat16 [2048, 5504], P('fs', 'tp'), may hold values from -0.125 to 0.125
- conv_weight: float32 [3, 5504], P(None, 'tp'), may hold values from -3 to 3
- conv_bias: float32 [5504], P('tp'), may hold values from -3 to 3
- down_weight: bfloat16 [5504, 2048], P('tp', 'fs'), may hold values from -0.078125 to 0.078125
Outputs:
- output: bfloat16 [49152, 2048], P(('fs', 'tp'))
All inputs are finite; a program needn't handle non-finite values.
Results may differ from a plain program's by a relative error of at most 0.012.
Values may be sent and summed in bfloat16 or wider, within the bound.
A program may use at most 128 MiB of HBM per device.

v0:
```python
import jax
import jax.numpy as jnp
from jax import lax
from jax.sharding import Mesh
from jax.sharding import PartitionSpec as P

FS_TP = ("fs_0", "fs_1", "tp")
FS = ("fs_0", "fs_1")


norm_eps = 1e-06


def sent_together(arrays, axis, dim, along):
    ends, at = ([], 0)
    for a in arrays[:-1]:
        at += a.shape[along]
        ends.append(at)
    both = jnp.concatenate(arrays, axis=along)
    return tuple(jnp.split(lax.all_gather(both, axis, axis=dim, tiled=True), ends, axis=along))


def whole_of(x, axes, dim):
    if not axes:
        return x
    nearer = lax.all_gather(x, axes[-1], axis=dim, tiled=True)
    return whole_of(nearer, axes[:-1], dim)


def body(
    mixed,
    residual,
    mix_weight,
    norm_gain,
    up_weight,
    gate_weight,
    conv_weight,
    conv_bias,
    down_weight,
):
    summed = jnp.dot(
        mixed,
        lax.all_gather(mix_weight, FS_TP, axis=0, tiled=True),
        preferred_element_type=jnp.float32,
    )
    stream = (residual.astype(jnp.float32) + summed).astype(jnp.bfloat16)
    x_float = stream.astype(jnp.float32)
    normed = (
        x_float
        * lax.rsqrt(jnp.mean(x_float * x_float, axis=-1, keepdims=True) + norm_eps)
        * norm_gain
    ).astype(jnp.bfloat16)
    half_cols = up_weight.shape[1]
    up_full, gate_full = sent_together((up_weight, gate_weight), FS, 0, 1)
    shard_piece = lax.all_gather(normed, "tp", axis=0, tiled=True)
    up_rows = jnp.dot(shard_piece, up_full, preferred_element_type=jnp.float32).astype(jnp.bfloat16)
    gate_rows = jnp.dot(shard_piece, gate_full, preferred_element_type=jnp.float32).astype(
        jnp.bfloat16
    )
    joined = jnp.concatenate([up_rows, gate_rows], axis=1)
    up_part = joined[:, :half_cols]
    gate_part = joined[:, half_cols:]
    up_float = lax.optimization_barrier(up_part).astype(jnp.float32)
    padded = jnp.pad(up_float, ((2, 0), (0, 0)))
    smoothed = (
        conv_bias
        + conv_weight[0] * padded[:-2]
        + conv_weight[1] * padded[1:-1]
        + conv_weight[2] * padded[2:]
    )
    hidden = (jax.nn.gelu(smoothed) * gate_part.astype(jnp.float32)).astype(jnp.bfloat16)
    down_full = whole_of(down_weight, FS, 1)
    summed_out = lax.psum_scatter(
        jnp.dot(hidden, down_full, preferred_element_type=jnp.float32).astype(jnp.bfloat16),
        "tp",
        scatter_dimension=0,
        tiled=True,
    ).astype(jnp.float32)
    return (x_float + summed_out).astype(jnp.bfloat16)


def solution(mesh):
    finer = Mesh(mesh.devices.reshape(4, 4, mesh.shape["tp"]), ("fs_0", "fs_1", "tp"))
    in_specs = (
        P(FS_TP, None),
        P(FS_TP, None),
        P(FS_TP, None),
        P(),
        P(FS, "tp"),
        P(FS, "tp"),
        P(None, "tp"),
        P("tp"),
        P("tp", FS),
    )
    out_specs = P(FS_TP, None)
    return jax.shard_map(body, mesh=finer, in_specs=in_specs, out_specs=out_specs, check_vma=False)
```

profile of v0, /device:TPU:1, one launch (start us, length us, event | category | flops | bytes accessed | tf_op | source)
XLA Modules:
  0.0 368.0 jit_solution(3910472219428671346)
XLA Ops:
  6.5 0.0 copy-start
  6.5 0.0 all-gather.5.cloned.1.call-start
  6.5 0.7 all-gather.5.cloned.1.call-update
  7.3 0.0 all-gather.9.cloned.1.call-start
  7.3 1.8 pad_maximum_fusion
  9.1 0.0 all-gather.9.cloned.1.call-update
  9.1 0.0 copy-start.2
  9.1 0.0 copy-start.1
  9.1 0.0 copy-start.3
  9.2 0.0 all-gather.7.cloned.1.call-start
  9.2 74.4 %all-gather.5.cloned.1.call-done = bf16[2048,2048]{1,0:T(8,128)(2,1)} async-done(((bf16[16,2048]{1,0:T(8,128)(2,1)}), bf16[2048,2048]{1,0:T(8,128)(2,1)}) %all-gather.5.cloned.1.call-update) | async-done | bytes 8388624 | tf_op jit(solution)/shard_map/all_gather | solution.py:43
  83.6 0.0 copy-done
  83.6 7.4 %fusion.15 = (f32[384]{0:T(512)S(1)}, bf16[384,2048]{1,0:T(8,128)(2,1)S(1)}) fusion(bf16[384,2048]{1,0:T(8,128)(2,1)S(1)} %copy-done, bf16[2048,2048]{1,0:T(8,128)(2,1)} %all-gather.5.cloned.1.call-done, bf16[384,2048]{1,0:T(8,128)(2,1)} %param.10), kind=kOutput, calls=%fused_computation.23 | convolution fusion | flops 3225943552 | bytes 13108736 | tf_op jit(solution)/shard_map/dot_general | solution.py:41
  91.0 0.0 copy-done.2
  91.0 1.6 fusion.17
  92.6 0.0 all-gather.7.cloned.1.call-update
  92.6 0.0 all-gather.11.cloned.1.call-start
  92.7 0.0 copy-done.1
  92.7 21.2 %all_gather.18 = bf16[688,512]{1,0:T(8,128)(2,1)} all-gather(bf16[688,128]{1,0:T(8,128)(2,1)S(1)} %copy-done.1), channel_id=1, replica_groups=mesh['fs_0'=4,'fs_1'=4,'tp'=8] {'fs_1'}, dimensions={1}, use_global_device_ids=true | all-gather | bytes 880640 | tf_op jit(solution)/shard_map/all_gather | solution.py:26
  113.9 0.0 all-gather.11.cloned.1.call-update
  113.9 0.2 reduce-scatter.2.cloned.1.call-start
  114.1 0.0 copy-done.3
  114.2 34.8 %all-gather.9.cloned.1.call-done = bf16[2048,1376]{0,1:T(8,128)(2,1)} async-done(((bf16[128,1376]{0,1:T(8,128)(2,1)}), bf16[2048,1376]{0,1:T(8,128)(2,1)}) %all-gather.9.cloned.1.call-update) | async-done | bytes 5636112 | tf_op jit(solution)/shard_map/all_gather | solution.py:20
  149.0 70.0 %all-gather.7.cloned.1.call-done = bf16[3072,2048]{1,0:T(8,128)(2,1)} async-done(((bf16[384,2048]{1,0:T(8,128)(2,1)}), bf16[3072,2048]{1,0:T(8,128)(2,1)}) %all-gather.7.cloned.1.call-update) | async-done | bytes 12582928 | tf_op jit(solution)/shard_map/all_gather | solution.py:55
  218.9 12.8 %convolution_convert_fusion.2 = bf16[3072,688]{0,1:T(8,128)(2,1)S(1)} fusion(bf16[3072,2048]{1,0:T(8,128)(2,1)} %all-gather.7.cloned.1.call-done, bf16[2048,1376]{0,1:T(8,128)(2,1)} %all-gather.9.cloned.1.call-done), kind=kOutput, calls=%fused_computation.19 | convolution fusion | flops 8659156992 | bytes 19628032 | tf_op jit(solution)/shard_map/dot_general | solution.py:56
  231.7 0.0 copy-start.4
  231.7 4.4 %convert_element_type.43 = f32[3072,688]{0,1:T(8,128)} convert(bf16[3072,688]{0,1:T(8,128)(2,1)S(1)} %convolution_convert_fusion.2) | non-fusion elementwise | flops 2113536 | bytes 12681216 | tf_op jit(solution)/shard_map/convert_element_type | solution.py:63
  236.1 21.2 %all-gather.11.cloned.1.call-done = bf16[688,2048]{1,0:T(8,128)(2,1)} async-done(((bf16[688,512]{1,0:T(8,128)(2,1)}), bf16[688,2048]{1,0:T(8,128)(2,1)}) %all-gather.11.cloned.1.call-update) | async-done | bytes 2818064 | tf_op jit(solution)/shard_map/all_gather | solution.py:26
  257.3 0.0 copy-done.4
  257.3 28.8 %convolution_convert_fusion = bf16[3072,2048]{1,0:T(8,128)(2,1)} fusion(bf16[688,2048]{1,0:T(8,128)(2,1)} %all-gather.11.cloned.1.call-done, f32[3072,688]{0,1:T(8,128)} %convert_element_type.43, f32[688]{0:T(1024)S(1)} %get-tuple-element.6, f32[688]{0:T(1024)S(1)} %get-tuple-element.7, f32[688]{0:T(1024)S(1)} %get-tuple-element.5, f32[688]{0:T(1024)S(1)} %copy-done.4, ...), kind=kOutput, calls=%fused_computation.1 | convolution fusion | flops 17358422016 | bytes 39267072 | tf_op jit(solution)/shard_map/dot_general | solution.py:74
  286.1 0.0 reduce-scatter.2.cloned.1.call-update
  286.1 72.1 %reduce-scatter.2.cloned.1.call-done = bf16[384,2048]{1,0:T(8,128)(2,1)} async-done(((bf16[3072,2048]{1,0:T(8,128)(2,1)}), bf16[384,2048]{1,0:T(8,128)(2,1)}) %reduce-scatter.2.cloned.1.call-update) | async-done | bytes 1572880 | tf_op jit(solution)/shard_map/reduce_scatter | solution.py:73
  358.2 3.2 fusion.18
  (2 shorter events, 0.0 us)
Async XLA Ops:
  6.5 77.1 %copy-start = (bf16[384,2048]{1,0:T(8,128)(2,1)S(1)}, bf16[384,2048]{1,0:T(8,128)(2,1)}, u32[]{:S(2)}) copy-start(bf16[384,2048]{1,0:T(8,128)(2,1)} %param.9) | copy-start | bytes 4718596
  6.5 77.1 %all-gather.5.cloned.1.call-start = ((), (), s32[]{:S(2)}) async-start(), calls=%async_computation.1 | async-start | bytes 8454144 | tf_op jit(solution)/shard_map/all_gather | solution.py:43
  7.3 141.7 %all-gather.9.cloned.1.call-start = ((), (), s32[]{:S(2)}) async-start(), calls=%async_computation.3 | async-start | bytes 5988352 | tf_op jit(solution)/shard_map/all_gather | solution.py:20
  9.1 81.9 %copy-start.2 = (f32[2048]{0:T(1024)S(1)}, f32[2048]{0:T(1024)}, u32[]{:S(2)}) copy-start(f32[2048]{0:T(1024)} %param.12) | copy-start | bytes 24580
  9.1 83.6 %copy-start.1 = (bf16[688,128]{1,0:T(8,128)(2,1)S(1)}, bf16[688,128]{1,0:T(8,128)(2,1)}, u32[]{:S(2)}) copy-start(bf16[688,128]{1,0:T(8,128)(2,1)} %param.17) | copy-start | bytes 528388
  9.1 105.0 %copy-start.3 = (f32[3,688]{1,0:T(4,128)S(1)}, f32[3,688]{1,0:T(4,128)}, u32[]{:S(2)}) copy-start(f32[3,688]{1,0:T(4,128)} %param.15) | copy-start | bytes 24772
  9.2 209.8 %all-gather.7.cloned.1.call-start = ((), (), s32[]{:S(2)}) async-start(), calls=%async_computation.2 | async-start | bytes 14155776 | tf_op jit(solution)/shard_map/all_gather | solution.py:55
  92.6 164.7 %all-gather.11.cloned.1.call-start = ((), (), s32[]{:S(2)}) async-start(), calls=%async_computation.4 | async-start | bytes 3522560 | tf_op jit(solution)/shard_map/all_gather | solution.py:26
  113.9 244.3 %reduce-scatter.2.cloned.1.call-start = ((), (), s32[]{:S(2)}) async-start(), calls=%async_computation.5 | async-start | bytes 14155776 | tf_op jit(solution)/shard_map/reduce_scatter | solution.py:73
  231.7 25.6 %copy-start.4 = (f32[688]{0:T(1024)S(1)}, f32[688]{0:T(1024)}, u32[]{:S(2)}) copy-start(f32[688]{0:T(1024)} %param.16) | copy-start | bytes 8260
Sparse Core Ops, SparseCore 0:
  10.3 73.2 all-gather.4
  85.7 63.1 all-gather.8
  150.7 68.2 all-gather.6
  220.5 36.7 all-gather.10
  286.2 71.9 reduce-scatter.1
where the time goes:
time: 368 us
  waiting for transfers between devices  273 us (74%)
  matrix products  48.9 us (13%)
  blocking collectives  21.2 us (6%)
  between operations  13.2 us (4%)
  other arithmetic  11 us (3%)
    all_gather x1, waiting for transfers between devices, body(): lax.all_gather(mix_weight, FS_TP, axis=0, tiled=True)  74.4 us
    reduce_scatter x1, waiting for transfers between devices, body(): lax.psum_scatter(jnp.dot(hidden, down_full, preferred_element_type=jnp.fl...  72.1 us
    all_gather x1, waiting for transfers between devices, body(): shard_piece = lax.all_gather(normed, 'tp', axis=0, tiled=True)  70 us
    all_gather x1, waiting for transfers between devices, sent_together(): lax.all_gather(both, axis, axis=dim, tiled=True)  34.8 us
    dot_general x1, matrix products, body(): jnp.dot(hidden, down_full, preferred_element_type=jnp.float32)  28.8 us
    all_gather x1, waiting for transfers between devices, whole_of(): nearer = lax.all_gather(x, axes[-1], axis=dim, tiled=True)  21.2 us
    all_gather x1, blocking collectives, whole_of(): nearer = lax.all_gather(x, axes[-1], axis=dim, tiled=True)  21.2 us
    dot_general x1, matrix products, body(): jnp.dot(shard_piece, up_full, preferred_element_type=jnp.float32)  12.8 us
  transfers between devices with their start and end apart: 5, of which 5 were waited for; matrix products, arithmetic and copies ran while one was open for 8% of the time, Pallas kernels for 0%

commit v1 on v0

v1 whole, which is shorter than its diff:
```python
import functools

import jax
import jax.numpy as jnp
from jax import lax
from jax.experimental import pallas as pl
from jax.experimental.pallas import tpu as pltpu
from jax.sharding import PartitionSpec as P

MESH = pl.DeviceIdType.MESH
F32 = jnp.float32
BF16 = jnp.bfloat16
NORM_EPS = 1e-06
GELU_C = 0.7978845608028654

D = 2048
TOK = 384
PIECE = 96
HALF = 192
UG = 1408
HID = 768


def gelu_tanh(v):
    return 0.5 * v * (1.0 + jnp.tanh(GELU_C * (v + 0.044715 * (v * v * v))))


class Gather:
    def __init__(self, ref, lo, rows, split, flip, fs, tp, send_sem, recv_sem):
        self.ref, self.lo, self.rows, self.split, self.flip = ref, lo, rows, split, flip
        self.tp, self.ss, self.rs = tp, send_sem, recv_sem
        z, y = fs // 4, fs % 4
        self.p = y * (1 - flip) + z * flip
        self.s = z * (1 - flip) + y * flip
        self.n = 0
        self.sends = []

    def zy(self, dp, ds):
        p, s = (self.p + dp + 4) % 4, (self.s + ds + 4) % 4
        return s * (1 - self.flip) + p * self.flip, p * (1 - self.flip) + s * self.flip

    def view(self, dp, ds, a=0, n=None):
        z, y = self.zy(dp, ds)
        n = self.rows if n is None else n
        return self.ref.at[z, y, pl.ds(self.lo + a, n)]

    def copy(self, k, blk, to):
        z, y = self.zy(*to)
        return pltpu.make_async_remote_copy(
            src_ref=blk, dst_ref=blk, send_sem=self.ss.at[self.n % 16], recv_sem=self.rs.at[k],
            device_id={"fs": z * 4 + y, "tp": self.tp}, device_id_type=MESH)

    def send(self, k, blk, to):
        c = self.copy(k, blk, to)
        c.start()
        self.sends.append(c)
        self.n += 1

    def wait(self, k, blk):
        self.copy(k, blk, (1, 0)).wait_recv()

    REL = (0, -1, 1, 2)

    def both(self, i):
        blk = self.view(self.REL[i], 0)
        self.send(4 + i, blk, (0, 1))
        self.send(8 + i, blk, (0, -1))

    def start(self):
        own = self.view(0, 0)
        self.send(0, own, (1, 0))
        self.send(1, own, (-1, 0))
        self.both(0)

    def near(self):
        s = self.split
        self.wait(0, self.view(-1, 0))
        self.send(2, self.view(-1, 0, 0, s), (1, 0))
        self.both(1)
        self.wait(1, self.view(1, 0))
        self.send(3, self.view(1, 0, s, self.rows - s), (-1, 0))
        self.both(2)

    def far(self):
        s = self.split
        self.wait(2, self.view(2, 0, 0, s))
        self.wait(3, self.view(2, 0, s, self.rows - s))
        self.both(3)

    def cross(self, i):
        below, above = self.view(self.REL[i], -1), self.view(self.REL[i], 1)
        self.wait(4 + i, below)
        if i < 2:
            self.send(12 + i, below, (0, 1))
        self.wait(8 + i, above)
        if i >= 2:
            self.send(12 + i, above, (0, -1))

    def last(self, i):
        self.wait(12 + i, self.view(self.REL[i], 2))

    def drain(self):
        for c in self.sends:
            c.wait_send()


def kernel(mixed, resid, wm_in, gain, ug_in, cw, dw_in, out,
           wm, ug, dwn, tok, mx, rs, stream, hal, xexp, hu, hid, pbuf, precv, xfwd, xfin,
           lsem, wx_s, wx_r, g_s, g_r, d_s, d_r, t_s, t_r, td_s, td_r, h_s, h_r, p_s, p_r,
           x_s, x_r):
    fs, tp = lax.axis_index("fs"), lax.axis_index("tp")
    z, y, x, c = fs // 4, fs % 4, tp // 2, tp % 2
    xr, xl, xo = (x + 1) % 4, (x + 3) % 4, (x + 2) % 4
    mate = x * 2 + (1 - c)
    drains = []

    def rcopy(src, dst, ss, rsem, tp_to, fs_to=None):
        return pltpu.make_async_remote_copy(
            src_ref=src, dst_ref=dst, send_sem=ss, recv_sem=rsem,
            device_id={"fs": fs if fs_to is None else fs_to, "tp": tp_to}, device_id_type=MESH)

    ld_ug = pltpu.make_async_copy(ug_in, ug.at[z, y], lsem.at[0])
    ld_dw = pltpu.make_async_copy(dw_in, dwn.at[z, y, pl.ds(0, 688)], lsem.at[1])
    ld_mx = pltpu.make_async_copy(mixed, mx, lsem.at[2])
    ld_rs = pltpu.make_async_copy(resid, rs, lsem.at[3])
    ld_mx.start()
    ld_rs.start()
    ld_ug.start()
    ld_dw.start()

    bar = pltpu.get_barrier_semaphore()
    peers = [(fs, (tp + k) % 8) for k in range(1, 8)]
    peers += [(z * 4 + (y + 1) % 4, tp), (z * 4 + (y + 3) % 4, tp)]
    peers += [(((z + 1) % 4) * 4 + y, tp), (((z + 3) % 4) * 4 + y, tp)]
    for f, t in peers:
        pl.semaphore_signal(bar, inc=1, device_id={"fs": f, "tp": t}, device_id_type=MESH)
    pl.semaphore_wait(bar, len(peers))

    half = tp // 4
    row16 = pl.multiple_of(tp * 16, 16)
    wm_dst = wm.at[z, y, pl.ds(row16, 16)]
    slot = tp % 4
    for k in range(1, 4):
        cp = rcopy(wm_in, wm_dst, wx_s.at[k], wx_r.at[slot], ((x + k) % 4) * 2 + half)
        cp.start()
        drains.append(cp)
    stay = pltpu.make_async_copy(wm_in, wm_dst, wx_r.at[slot])
    over = rcopy(wm_in, wm_dst, wx_s.at[0], wx_r.at[slot], mate)

    @pl.when(c == half)
    def _():
        stay.start()

    @pl.when(c != half)
    def _():
        over.start()

    zero_rows = jnp.zeros((HID - 688, 128), BF16)

    @pl.loop(0, 16)
    def _(f):
        dwn[f // 4, f % 4, pl.ds(688, HID - 688)] = zero_rows

    lo = pl.multiple_of(c * 64, 64)
    for k in range(4):
        row = pl.multiple_of(lo + k * 16, 16)
        blk = wm.at[z, y, pl.ds(row, 16)]
        rcopy(blk, blk, wx_s.at[0], wx_r.at[k], mate).wait_recv()

    gw = Gather(wm, lo, 64, 32, c, fs, tp, g_s.at[0], g_r.at[0])
    gu = Gather(ug, 0, 128, 64, c, fs, tp, g_s.at[1], g_r.at[1])
    gd = Gather(dwn, 0, 688, 352, 1 - c, fs, tp, g_s.at[2], g_r.at[2])

    def share(k, dp, ds):
        blk = gw.view(dp, ds)
        cp = rcopy(blk, blk, d_s.at[k], d_r.at[k], mate)
        cp.start()
        drains.append(cp)

    gw.start()
    share(0, 0, 0)
    gw.near()
    share(1, -1, 0)
    share(2, 1, 0)
    gw.cross(0)
    share(4, 0, -1)
    share(5, 0, 1)
    gw.far()
    share(3, 2, 0)
    gw.cross(1)
    share(6, -1, -1)
    share(7, -1, 1)
    gw.cross(2)
    share(8, 1, -1)
    share(9, 1, 1)
    gw.cross(3)
    share(10, 2, -1)
    share(11, 2, 1)
    ld_ug.wait()
    gu.start()
    for i in range(4):
        gw.last(i)
        share(12 + i, gw.REL[i], 2)
    other = pl.multiple_of(64 - lo, 64)
    for k in range(16):
        blk = wm.at[k // 4, k % 4, pl.ds(other, 64)]
        rcopy(blk, blk, d_s.at[k], d_r.at[k], mate).wait_recv()

    ld_mx.wait()
    ld_rs.wait()

    @pl.loop(0, 8)
    def _(n):
        cols = pl.ds(pl.multiple_of(n * 256, 256), 256)
        w = wm[:, :, :, cols].reshape(D, 256)
        s = jnp.dot(mx[...], w, preferred_element_type=F32)
        stream[:, cols] = (rs[:, cols].astype(F32) + s).astype(BF16)

    def send_tok(k, piece, xsrc, to_right, sidx):
        blk = tok.at[xsrc, c, piece]
        side = 0 if to_right else 1
        cp = rcopy(blk, blk, t_s.at[side, sidx], t_r.at[side, sidx],
                   (xr if to_right else xl) * 2 + c)
        cp.start()
        drains.append(cp)

    def norm_piece(k):
        @pl.loop(0, PIECE // 16)
        def _(r):
            rows = pl.ds(pl.multiple_of(k * PIECE + r * 16, 16), 16)
            v = stream[rows, :].astype(F32)
            m = jnp.mean(v * v, axis=-1, keepdims=True)
            v = v * lax.rsqrt(m + NORM_EPS) * gain[...]
            tok[x, c, k, pl.ds(pl.multiple_of(r * 16, 16), 16), :] = v.astype(BF16)

    norm_piece(0)
    send_tok(0, 0, x, True, 0)
    norm_piece(2)
    send_tok(2, 2, x, False, 0)
    norm_piece(1)
    send_tok(1, 1, x, True, 1)
    norm_piece(3)
    send_tok(3, 3, x, False, 1)

    tails = []
    for k in (1, 3):
        v = tok[x, c, k, pl.ds(PIECE - 16, 16), :].astype(F32)
        for r in (14, 15):
            for q in range(8):
                tails.append(v[r:r + 1, q * 256:(q + 1) * 256])
    hal[tp] = jnp.concatenate(tails, axis=0).astype(BF16)
    for k in range(1, 8):
        cp = rcopy(hal.at[tp], hal.at[tp], h_s.at[k], h_r.at[8 - k], (tp + k) % 8)
        cp.start()
        drains.append(cp)

    def mate_tok(k, xsrc, first, n):
        blk = tok.at[xsrc, c, pl.ds(first, n)]
        cp = rcopy(blk, blk, td_s.at[k], td_r.at[k], mate)
        cp.start()
        drains.append(cp)

    def mate_wait(k, xsrc, first, n):
        blk = tok.at[xsrc, 1 - c, pl.ds(first, n)]
        rcopy(blk, blk, td_s.at[k], td_r.at[k], mate).wait_recv()

    def tok_wait(from_left, idx, xsrc, piece):
        blk = tok.at[xsrc, c, piece]
        side = 0 if from_left else 1
        rcopy(blk, blk, t_s.at[side, idx], t_r.at[side, idx], mate).wait_recv()

    mate_tok(0, x, 0, 4)
    gu.near()
    gu.cross(0)
    gu.far()

    tok_wait(True, 0, xl, 0)
    send_tok(0, 0, xl, True, 2)
    tok_wait(False, 0, xr, 2)
    send_tok(2, 2, xr, False, 2)
    gu.cross(1)
    gu.cross(2)
    tok_wait(True, 1, xl, 1)
    send_tok(1, 1, xl, True, 3)
    send_tok(2, 2, x, True, 4)
    send_tok(3, 3, x, True, 5)
    tok_wait(False, 1, xr, 3)
    send_tok(3, 3, xr, False, 3)
    send_tok(0, 0, x, False, 4)
    send_tok(1, 1, x, False, 5)
    mate_tok(1, xl, 0, 2)
    mate_tok(2, xr, 2, 2)
    gu.cross(3)
    ld_dw.wait()
    gd.start()
    for i in range(4):
        gu.last(i)

    for k in range(1, 8):
        src = (tp + k) % 8
        rcopy(hal.at[src], hal.at[src], h_s.at[k], h_r.at[k], mate).wait_recv()
    hv = hal[...].reshape(256, 256).astype(F32)
    rid = lax.broadcasted_iota(jnp.int32, (256, 256), 0) % 8
    for q in range(8):
        xexp[:, q * 256:(q + 1) * 256] = jnp.where(rid == q, hv, 0.0).astype(BF16)

    gd.near()
    gd.cross(0)
    gd.far()

    @pl.loop(0, 6)
    def _(i):
        w = ug[:, :, :, pl.ds(pl.multiple_of(i * 256, 256), 128)].reshape(D, 128)
        r = jnp.dot(xexp[...], w, preferred_element_type=F32)
        r = jnp.sum(r.reshape(32, 8, 128), axis=1).astype(BF16).astype(F32)
        cols = pl.ds(pl.multiple_of(i * 128, 128), 128)
        hu[0, 0:2, cols] = jnp.zeros((2, 128), F32)
        for q in range(15):
            hu[q + 1, 0:2, cols] = r[2 * q:2 * q + 2]

    gd.cross(1)
    gd.cross(2)
    gd.cross(3)

    tok_wait(True, 2, xo, 0)
    tok_wait(True, 3, xo, 1)
    mate_tok(3, xo, 0, 2)
    tok_wait(False, 2, xo, 2)
    tok_wait(False, 3, xo, 3)
    mate_tok(4, xo, 2, 2)
    for i in range(4):
        gd.last(i)
    mate_wait(1, xl, 0, 2)
    mate_wait(2, xr, 2, 2)
    mate_wait(3, xo, 0, 2)
    mate_wait(4, xo, 2, 2)

    rowid = lax.broadcasted_iota(jnp.int32, (HALF, 128), 0)

    def unit(xx, cc, h, cls):
        j = xx * 2 + cc

        def act(i, u, g):
            cols = pl.ds(pl.multiple_of(i * 128, 128), 128)
            u = u.astype(BF16).astype(F32)
            g = g.astype(BF16).astype(F32)
            before = hu[j * 2 + h, :, cols]
            h0, h1 = before[0:1], before[1:2]
            u1 = jnp.where(rowid == 0, h1, pltpu.roll(u, 1, 0))
            u2 = jnp.where(rowid == 0, h0, jnp.where(rowid == 1, h1, pltpu.roll(u, 2, 0)))
            s = (cw[pl.ds(3, 1), cols] + cw[pl.ds(0, 1), cols] * u2
                 + cw[pl.ds(1, 1), cols] * u1 + cw[pl.ds(2, 1), cols] * u)
            hid[:, cols] = (gelu_tanh(s) * g).astype(BF16)

        def rows():
            return tok[xx, cc, pl.ds(h * 2, 2)].reshape(HALF, D)

        @pl.loop(0, 5)
        def _(i):
            w = ug[:, :, :, pl.ds(pl.multiple_of(i * 256, 256), 256)].reshape(D, 256)
            r = jnp.dot(rows(), w, preferred_element_type=F32)
            act(i, r[:, :128], r[:, 128:])

        w = ug[:, :, :, pl.ds(1280, 128)].reshape(D, 128)
        r = jnp.dot(rows(), w, preferred_element_type=F32)
        act(5, r, pltpu.roll(r, 64, 1))

        @pl.loop(0, 8)
        def _(n):
            zz, y0 = n // 2, (n % 2) * 2
            w = jnp.concatenate([dwn[zz, y0], dwn[zz, y0 + 1]], axis=1)
            r = jnp.dot(hid[...], w, preferred_element_type=F32)
            pbuf[cls, xx, h, :, pl.ds(pl.multiple_of(n * 256, 256), 256)] = r.astype(BF16)

    def group(xs, hs):
        @pl.loop(0, 4)
        def _(i):
            cls, kind = i // 2, i % 2
            cc = (1 - c) * (1 - cls) + c * cls
            xx = xs[0] * (1 - kind) + xs[1] * kind
            h = hs[0] * (1 - kind) + hs[1] * kind
            unit(xx, cc, h, cls)

            @pl.when(cls == 0)
            def _():
                rcopy(pbuf.at[0, xx, h], precv.at[xx, h], p_s.at[xx, h], p_r.at[xx, h],
                      mate).start()

    def joined(xx, h, extra=None):
        rcopy(pbuf.at[0, xx, h], precv.at[xx, h], p_s.at[xx, h], p_r.at[xx, h], mate).wait_recv()

        @pl.loop(0, HALF // 16)
        def _(r):
            rr = pl.ds(pl.multiple_of(r * 16, 16), 16)
            v = pbuf[1, xx, h, rr, :].astype(F32) + precv[xx, h, rr, :].astype(F32)
            if extra is not None:
                v = v + extra[rr, :].astype(F32)
            pbuf[1, xx, h, rr, :] = v.astype(BF16)

    def send_sum(xx, h, to_right, dst, k):
        side = 0 if to_right else 1
        cp = rcopy(pbuf.at[1, xx, h], dst, x_s.at[side, k], x_r.at[side, k],
                   (xr if to_right else xl) * 2 + c)
        cp.start()
        drains.append(cp)

    def wait_sum(from_left, dst, k):
        side = 0 if from_left else 1
        rcopy(dst, dst, x_s.at[side, k], x_r.at[side, k], mate).wait_recv()

    group((xo, xo), (0, 1))
    joined(xo, 0)
    send_sum(xo, 0, True, xfwd.at[0], 0)
    joined(xo, 1)
    send_sum(xo, 1, False, xfwd.at[1], 0)
    group((xr, xl), (1, 0))
    joined(xr, 1)
    send_sum(xr, 1, True, xfin.at[0, 1], 1)
    joined(xl, 0)
    send_sum(xl, 0, False, xfin.at[1, 0], 1)

    tok_wait(True, 4, xl, 2)
    tok_wait(True, 5, xl, 3)
    mate_tok(5, xl, 2, 2)
    tok_wait(False, 4, xr, 0)
    tok_wait(False, 5, xr, 1)
    mate_tok(6, xr, 0, 2)
    mate_wait(5, xl, 2, 2)
    mate_wait(6, xr, 0, 2)
    group((xr, xl), (0, 1))
    wait_sum(True, xfwd.at[0], 0)
    joined(xr, 0, xfwd.at[0])
    send_sum(xr, 0, True, xfin.at[0, 0], 2)
    wait_sum(False, xfwd.at[1], 0)
    joined(xl, 1, xfwd.at[1])
    send_sum(xl, 1, False, xfin.at[1, 1], 2)

    mate_wait(0, x, 0, 4)
    group((x, x), (0, 1))
    joined(x, 0)
    joined(x, 1)

    wait_sum(True, xfin.at[0, 1], 1)
    wait_sum(False, xfin.at[1, 0], 1)
    wait_sum(True, xfin.at[0, 0], 2)
    wait_sum(False, xfin.at[1, 1], 2)
    for h in range(2):
        @pl.loop(0, HALF // 16)
        def _(r):
            rr = pl.ds(pl.multiple_of(r * 16, 16), 16)
            oo = pl.ds(pl.multiple_of(h * HALF + r * 16, 16), 16)
            v = stream[oo, :].astype(F32) + pbuf[1, x, h, rr, :].astype(F32)
            v = v + xfin[0, h, rr, :].astype(F32) + xfin[1, h, rr, :].astype(F32)
            out[oo, :] = v.astype(BF16)

    @pl.when(c == half)
    def _():
        pass

    @pl.when(c != half)
    def _():
        over.wait_send()

    for cp in drains:
        cp.wait_send()
    gw.drain()
    gu.drain()
    gd.drain()
    for xx in range(4):
        for h in range(2):
            rcopy(pbuf.at[0, xx, h], precv.at[xx, h], p_s.at[xx, h], p_r.at[xx, h],
                  mate).wait_send()


def body(mixed, residual, mix_weight, norm_gain, up_weight, gate_weight, conv_weight, conv_bias,
         down_weight):
    parts = []
    for i in range(5):
        parts += [up_weight[:, i * 128:(i + 1) * 128], gate_weight[:, i * 128:(i + 1) * 128]]
    gap = jnp.zeros((128, 16), BF16)
    parts += [up_weight[:, 640:], gap, gate_weight[:, 640:], gap]
    ug_own = jnp.concatenate(parts, axis=1)
    taps = jnp.concatenate([conv_weight, conv_bias[None], jnp.zeros((4, 688), F32)], axis=0)
    taps = jnp.pad(taps, ((0, 0), (0, HID - 688)))

    any_ = pl.BlockSpec(memory_space=pl.ANY)
    vm = pl.BlockSpec(memory_space=pltpu.VMEM)
    dma = pltpu.SemaphoreType.DMA
    return pl.pallas_call(
        kernel,
        out_shape=jax.ShapeDtypeStruct((TOK, D), BF16),
        in_specs=[any_, any_, any_, vm, any_, vm, any_],
        out_specs=vm,
        scratch_shapes=[
            pltpu.VMEM((4, 4, 128, D), BF16),
            pltpu.VMEM((4, 4, 128, UG), BF16),
            pltpu.VMEM((4, 4, HID, 128), BF16),
            pltpu.VMEM((4, 2, 4, PIECE, D), BF16),
            pltpu.VMEM((TOK, D), BF16),
            pltpu.VMEM((TOK, D), BF16),
            pltpu.VMEM((TOK, D), BF16),
            pltpu.VMEM((8, 32, 256), BF16),
            pltpu.VMEM((256, D), BF16),
            pltpu.VMEM((16, 8, HID), F32),
            pltpu.VMEM((HALF, HID), BF16),
            pltpu.VMEM((2, 4, 2, HALF, D), BF16),
            pltpu.VMEM((4, 2, HALF, D), BF16),
            pltpu.VMEM((2, HALF, D), BF16),
            pltpu.VMEM((2, 2, HALF, D), BF16),
            dma((4,)), dma((4,)), dma((4,)),
            dma((3, 16)), dma((3, 16)),
            dma((16,)), dma((16,)),
            dma((2, 6)), dma((2, 6)),
            dma((7,)), dma((7,)),
            dma((8,)), dma((8,)),
            dma((4, 2)), dma((4, 2)),
            dma((2, 3)), dma((2, 3)),
        ],
        compiler_params=pltpu.CompilerParams(
            collective_id=0, has_side_effects=True, vmem_limit_bytes=67_043_328),
    )(mixed, residual, mix_weight, norm_gain[None], ug_own, taps, down_weight)


def solution(mesh):
    rows = P(("fs", "tp"), None)
    in_specs = (rows, rows, rows, P(), P("fs", "tp"), P("fs", "tp"), P(None, "tp"), P("tp"),
                P("tp", "fs"))
    return jax.shard_map(body, mesh=mesh, in_specs=in_specs, out_specs=rows, check_vma=False)
```

time: 368 us -> 189 us (0.51)
  waiting for transfers between devices: 273 us -> 0 us
  Pallas kernels: 0 us -> 179 us
  matrix products: 48.9 us -> 0 us
  blocking collectives: 21.2 us -> 0 us
  between operations: 13.2 us -> 0.09 us
  other arithmetic: 11 us -> 0.79 us
  local copies, waits for them, and re-layouts: 0.06 us -> 9.48 us
    all_gather x4 -> x0, waiting for transfers between devices: 200 us -> none  [the longest x1 74.4 us: body(): lax.all_gather(mix_weight, FS_TP, axis=0, tiled=True)]
    pallas_call x0 -> x1, Pallas kernels: none -> 179 us  [body(): pl.pallas_call(kernel, out_shape=jax.ShapeDtypeStruct((TOK, D), BF16), in...]
    reduce_scatter x1 -> x0, waiting for transfers between devices: 72.1 us -> none  [body(): lax.psum_scatter(jnp.dot(hidden, down_full, preferred_element_type=jnp.fl...]
    dot_general x3 -> x0, matrix products: 48.9 us -> none  [the longest x1 28.8 us: body(): jnp.dot(hidden, down_full, preferred_element_type=jnp.float32)]
    all_gather x1 -> x0, blocking collectives: 21.2 us -> none  [whole_of(): nearer = lax.all_gather(x, axes[-1], axis=dim, tiled=True)]
    convert_element_type x3 -> x0, other arithmetic: 9.18 us -> none  [the longest x1 4.39 us: body(): up_float = lax.optimization_barrier(up_part).astype(jnp.float32)]
    unnamed x10 -> x13, local copies, waits for them, and re-layouts: 0.03 us -> 4.15 us
  transfers between devices with their start and end apart: 5 -> 0, of which waited for: 5 -> 0; matrix products, arithmetic and copies ran while one was open for 8% -> 0% of each run, Pallas kernels for 0% -> 0%
where the time goes in v1:
time: 189 us
  Pallas kernels  179 us (95%)
  local copies, waits for them, and re-layouts  9.48 us (5%)
    pallas_call x1, Pallas kernels, body(): pl.pallas_call(kernel, out_shape=jax.ShapeDtypeStruct((TOK, D), BF16), in...  179 us
    unnamed x13, local copies, waits for them, and re-layouts  4.15 us

profile of v1, /device:TPU:1, one launch (start us, length us, event | category | flops | bytes accessed | tf_op | source)
XLA Modules:
  0.0 188.9 jit_solution(2326374920337007381)
XLA Ops:
  0.0 0.1 pad.7.clone
  0.1 0.7 broadcast_in_dim.14
  0.8 0.7 slice.46
  1.5 0.7 slice.47
  2.2 0.1 copy.33
  2.3 0.1 copy.32
  2.4 0.8 maximum_maximum_fusion
  3.2 0.6 pad.4.cw
  3.8 0.8 fusion.1
  4.7 0.1 copy.30
  4.8 0.1 copy.28
  4.9 0.1 copy.26
  5.0 0.1 copy.24
  5.2 0.1 copy.22
  5.3 0.8 fusion
  6.1 0.1 copy.31
  6.2 0.1 copy.29
  6.4 0.1 copy.27
  6.5 0.1 copy.25
  6.6 0.1 copy.23
  6.8 0.9 concatenate.6.ug_in
  7.6 178.6 %shard_map.91 = bf16[384,2048]{1,0:T(8,128)(2,1)} custom-call(bf16[384,2048]{1,0:T(8,128)(2,1)} %mixed.1, bf16[384,2048]{1,0:T(8,128)(2,1)} %resid.1, bf16[16,2048]{1,0:T(8,128)(2,1)} %wm_in.1, f32[1,2048]{1,0:T(1,128)} %bitcast.1, bf16[128,1408]{1,0:T(8,128)(2,1)} %concatenate.6.ug_in, f32[8,768]{1,0:T(8,128)} %pad.4.cw, bf16[688,128]{1,0:T(8,128)(2,1)} %dw_in.1), custom_call_target="tpu_custom_call" | custom-call | tf_op jit(solution)/shard_map/pallas_call | solution.py:489
  186.2 2.7 %copy.35 = bf16[384,2048]{1,0:T(8,128)(2,1)} copy(bf16[384,2048]{1,0:T(8,128)(2,1)} %shard_map.91) | data formatting | bytes 3145728
  (2 shorter events, 0.0 us)

commit v2 on v1

v2 whole, which is shorter than its diff:
```python
import functools

import jax
import jax.numpy as jnp
from jax import lax
from jax.experimental import pallas as pl
from jax.experimental.pallas import tpu as pltpu
from jax.sharding import PartitionSpec as P

MESH = pl.DeviceIdType.MESH
F32 = jnp.float32
BF16 = jnp.bfloat16
NORM_EPS = 1e-06
GELU_C = 0.7978845608028654

D = 2048
TOK = 384
CH = 1024
HALF = 192
UG = 1408
HID = 768


def gated_gelu(v, gate):
    t = jnp.tanh(v * (GELU_C + (GELU_C * 0.044715) * (v * v)))
    v = 0.5 * v
    return (v + v * t) * gate


class Phases:
    def __init__(self):
        self.scope = None

    def __call__(self, name):
        if self.scope is not None:
            self.scope.__exit__(None, None, None)
        self.scope = jax.named_scope(name) if name else None
        if name:
            self.scope.__enter__()


class Gather:
    def __init__(self, ref, lo, rows, split, flip, fs, tp, send_sem, recv_sem):
        self.ref, self.lo, self.rows, self.split, self.flip = ref, lo, rows, split, flip
        self.tp, self.ss, self.rs = tp, send_sem, recv_sem
        z, y = fs // 4, fs % 4
        self.p = y * (1 - flip) + z * flip
        self.s = z * (1 - flip) + y * flip
        self.n = 0
        self.sends = []

    def zy(self, dp, ds):
        p, s = (self.p + dp + 4) % 4, (self.s + ds + 4) % 4
        return s * (1 - self.flip) + p * self.flip, p * (1 - self.flip) + s * self.flip

    def view(self, dp, ds, a=0, n=None):
        z, y = self.zy(dp, ds)
        n = self.rows if n is None else n
        return self.ref.at[z, y, pl.ds(self.lo + a, n)]

    def copy(self, k, blk, to):
        z, y = self.zy(*to)
        return pltpu.make_async_remote_copy(
            src_ref=blk, dst_ref=blk, send_sem=self.ss.at[self.n % 16], recv_sem=self.rs.at[k],
            device_id={"fs": z * 4 + y, "tp": self.tp}, device_id_type=MESH)

    def send(self, k, blk, to):
        c = self.copy(k, blk, to)
        c.start()
        self.sends.append(c)
        self.n += 1

    def wait(self, k, blk):
        self.copy(k, blk, (1, 0)).wait_recv()

    REL = (0, -1, 1, 2)

    def both(self, i):
        blk = self.view(self.REL[i], 0)
        self.send(4 + i, blk, (0, 1))
        self.send(8 + i, blk, (0, -1))

    def start(self):
        own = self.view(0, 0)
        self.send(0, own, (1, 0))
        self.send(1, own, (-1, 0))
        self.both(0)

    def near(self):
        s = self.split
        self.wait(0, self.view(-1, 0))
        self.send(2, self.view(-1, 0, 0, s), (1, 0))
        self.both(1)
        self.wait(1, self.view(1, 0))
        self.send(3, self.view(1, 0, s, self.rows - s), (-1, 0))
        self.both(2)

    def far(self):
        s = self.split
        self.wait(2, self.view(2, 0, 0, s))
        self.wait(3, self.view(2, 0, s, self.rows - s))
        self.both(3)

    def cross(self, i):
        below, above = self.view(self.REL[i], -1), self.view(self.REL[i], 1)
        self.wait(4 + i, below)
        if i < 2:
            self.send(12 + i, below, (0, 1))
        self.wait(8 + i, above)
        if i >= 2:
            self.send(12 + i, above, (0, -1))

    def last(self, i):
        self.wait(12 + i, self.view(self.REL[i], 2))

    def drain(self):
        for c in self.sends:
            c.wait_send()


def kernel(mixed, resid, wm_in, gain, up_in, gate_in, cw_in, cb_in, dw_in, out, xfin,
           wm, ug, dwn, upt, cw, tok, rr, mx, rs, hal, xexp, hu, hid, pbuf, precv, xfwd, base,
           lsem, wx_s, wx_r, g_s, g_r, d_s, d_r, t_s, t_r, td_s, td_r, rd_s, rd_r, h_s, h_r,
           p_s, p_r, x_s, x_r):
    fs, tp = lax.axis_index("fs"), lax.axis_index("tp")
    z, y, x, c = fs // 4, fs % 4, tp // 2, tp % 2
    xr, xl, xo = (x + 1) % 4, (x + 3) % 4, (x + 2) % 4
    mate = x * 2 + (1 - c)
    drains = []

    def rcopy(src, dst, ss, rsem, tp_to, fs_to=None):
        return pltpu.make_async_remote_copy(
            src_ref=src, dst_ref=dst, send_sem=ss, recv_sem=rsem,
            device_id={"fs": fs if fs_to is None else fs_to, "tp": tp_to}, device_id_type=MESH)

    ph = Phases()
    ph("load")
    ld_up = pltpu.make_async_copy(up_in, upt.at[0], lsem.at[0])
    ld_gate = pltpu.make_async_copy(gate_in, upt.at[1], lsem.at[4])
    ld_dw = pltpu.make_async_copy(dw_in, dwn.at[z, y, pl.ds(0, 688)], lsem.at[1])
    ld_mx = pltpu.make_async_copy(mixed, mx, lsem.at[2])
    ld_rs = pltpu.make_async_copy(resid, rs, lsem.at[3])
    ld_up.start()
    ld_gate.start()
    ld_mx.start()
    ld_rs.start()
    ld_dw.start()

    ph("barrier")
    bar = pltpu.get_barrier_semaphore()
    peers = [(fs, (tp + k) % 8) for k in range(1, 8)]
    peers += [(z * 4 + (y + 1) % 4, tp), (z * 4 + (y + 3) % 4, tp)]
    peers += [(((z + 1) % 4) * 4 + y, tp), (((z + 3) % 4) * 4 + y, tp)]
    for f, t in peers:
        pl.semaphore_signal(bar, inc=1, device_id={"fs": f, "tp": t}, device_id_type=MESH)
    pl.semaphore_wait(bar, len(peers))

    ph("wx")
    half = tp // 4
    row16 = pl.multiple_of(tp * 16, 16)
    slot = tp % 4
    stays, overs = [], []
    for ch in range(2):
        src = wm_in.at[:, pl.ds(ch * CH, CH)]
        dst = wm.at[ch, z, y, pl.ds(row16, 16)]
        for k in range(1, 4):
            cp = rcopy(src, dst, wx_s.at[ch, k], wx_r.at[ch, slot], ((x + k) % 4) * 2 + half)
            cp.start()
            drains.append(cp)
        stays.append(pltpu.make_async_copy(src, dst, wx_r.at[ch, slot]))
        overs.append(rcopy(src, dst, wx_s.at[ch, 0], wx_r.at[ch, slot], mate))

    @pl.when(c == half)
    def _():
        for cp in stays:
            cp.start()

    @pl.when(c != half)
    def _():
        for cp in overs:
            cp.start()

    lo = pl.multiple_of(c * 64, 64)
    other = pl.multiple_of(64 - lo, 64)
    gws = [Gather(wm.at[ch], lo, 64, 32, c, fs, tp, g_s.at[ch], g_r.at[ch]) for ch in range(2)]
    gw, gv = gws
    gu = Gather(ug, 0, 128, 64, c, fs, tp, g_s.at[2], g_r.at[2])
    gd = Gather(dwn, 0, 688, 352, 1 - c, fs, tp, g_s.at[3], g_r.at[3])

    def share(ch, k, dp, ds):
        blk = gws[ch].view(dp, ds)
        cp = rcopy(blk, blk, d_s.at[ch, k], d_r.at[ch, k], mate)
        cp.start()
        drains.append(cp)

    def shared(ch):
        for k in range(16):
            blk = wm.at[ch, k // 4, k % 4, pl.ds(other, 64)]
            rcopy(blk, blk, d_s.at[ch, k], d_r.at[ch, k], mate).wait_recv()

    def w_start(ch):
        for k in range(4):
            row = pl.multiple_of(lo + k * 16, 16)
            blk = wm.at[ch, z, y, pl.ds(row, 16)]
            rcopy(blk, blk, wx_s.at[ch, 0], wx_r.at[ch, k], mate).wait_recv()
        gws[ch].start()
        share(ch, 0, 0, 0)

    def w_near(ch):
        gws[ch].near()
        share(ch, 1, -1, 0)
        share(ch, 2, 1, 0)

    def w_far(ch):
        gws[ch].far()
        share(ch, 3, 2, 0)

    def w_cross(ch, i):
        gws[ch].cross(i)
        share(ch, 4 + 2 * i, Gather.REL[i], -1)
        share(ch, 5 + 2 * i, Gather.REL[i], 1)

    def w_last(ch):
        for i in range(4):
            gws[ch].last(i)
            share(ch, 12 + i, Gather.REL[i], 2)

    ph("w_start")
    w_start(0)
    w_start(1)

    ph("prep")
    zero_rows = jnp.zeros((HID - 688, 128), BF16)

    @pl.loop(0, 16)
    def _(f):
        dwn[f // 4, f % 4, pl.ds(688, HID - 688)] = zero_rows

    cw[...] = jnp.zeros((8, HID), F32)
    cw[0:3, 0:688] = cw_in[...]
    cw[3:4, 0:688] = cb_in[...].reshape(1, 688)
    ld_up.wait()
    ld_gate.wait()
    gn = gain[:, pl.ds(pl.multiple_of(fs * 128, 128), 128)]
    for i in range(5):
        for k in range(2):
            t = upt[k, pl.ds(i * 128, 128), :].astype(F32) * gn
            ug[z, y, :, pl.ds(i * 256 + k * 128, 128)] = t.T.astype(BF16)
    gap = jnp.zeros((16, 128), F32)
    t = [upt[0, pl.ds(640, 48), :].astype(F32) * gn, gap,
         upt[1, pl.ds(640, 48), :].astype(F32) * gn, gap]
    ug[z, y, :, pl.ds(1280, 128)] = jnp.concatenate(t, axis=0).T.astype(BF16)

    def mix(ch, n):
        w = wm[ch, :, :, :, n * 512:(n + 1) * 512].reshape(D, 512)
        s = jnp.dot(mx[...], w, preferred_element_type=F32)
        at = ch * CH + n * 512
        s = rs[:, at:at + 512].astype(F32) + s
        tok[x, c, ch, :, n * 512:(n + 1) * 512] = s.astype(BF16)

    def send_tok(xsrc, h, ch, to_right, sidx):
        blk = tok.at[xsrc, c, ch, pl.ds(h * HALF, HALF)]
        side = 0 if to_right else 1
        cp = rcopy(blk, blk, t_s.at[side, sidx], t_r.at[side, sidx],
                   (xr if to_right else xl) * 2 + c)
        cp.start()
        drains.append(cp)

    def tok_wait(from_left, idx, xsrc, h, ch):
        blk = tok.at[xsrc, c, ch, pl.ds(h * HALF, HALF)]
        side = 0 if from_left else 1
        rcopy(blk, blk, t_s.at[side, idx], t_r.at[side, idx], mate).wait_recv()

    def factor(xsrc, h):
        acc = None
        for ch in range(2):
            for k in range(CH // 128):
                v = tok[xsrc, c, ch, h * HALF:(h + 1) * HALF, k * 128:(k + 1) * 128].astype(F32)
                acc = v * v if acc is None else acc + v * v
        m = jnp.sum(acc, axis=-1, keepdims=True) * (1.0 / D)
        rr[xsrc, c, h] = jnp.broadcast_to(lax.rsqrt(m + NORM_EPS), (HALF, 128))

    def to_mate(k, xsrc, h):
        blk = tok.at[xsrc, c, :, pl.ds(h * HALF, HALF)]
        cp = rcopy(blk, blk, td_s.at[k], td_r.at[k], mate)
        cp.start()
        drains.append(cp)
        factor(xsrc, h)
        blk = rr.at[xsrc, c, h]
        cp = rcopy(blk, blk, rd_s.at[k], rd_r.at[k], mate)
        cp.start()
        drains.append(cp)

    def mate_wait(k, xsrc, h):
        blk = tok.at[xsrc, 1 - c, :, pl.ds(h * HALF, HALF)]
        rcopy(blk, blk, td_s.at[k], td_r.at[k], mate).wait_recv()
        blk = rr.at[xsrc, 1 - c, h]
        rcopy(blk, blk, rd_s.at[k], rd_r.at[k], mate).wait_recv()

    ph("w0_near")
    w_near(0)
    ph("w0_c0")
    w_cross(0, 0)
    ph("w0_far")
    w_far(0)
    ph("w1_near")
    w_near(1)
    ph("w0_c1")
    w_cross(0, 1)
    ph("w0_c2")
    w_cross(0, 2)
    ph("w1_c0")
    w_cross(1, 0)
    ph("w1_far")
    w_far(1)
    ph("w0_c3")
    w_cross(0, 3)
    ph("w1_c1")
    w_cross(1, 1)
    ph("w0_last")
    w_last(0)
    ph("w0_shared")
    shared(0)
    ld_mx.wait()
    ld_rs.wait()
    ph("mix0")
    mix(0, 0)
    ph("w1_c2")
    w_cross(1, 2)
    ph("mix1")
    mix(0, 1)
    send_tok(x, 0, 0, True, 0)
    send_tok(x, 1, 0, False, 0)
    send_tok(x, 1, 0, True, 1)
    send_tok(x, 0, 0, False, 1)
    ph("w1_c3")
    w_cross(1, 3)
    gu.start()
    ph("w1_last")
    w_last(1)
    ph("w1_shared")
    shared(1)
    ph("mix2")
    mix(1, 0)
    mix(1, 1)
    ph("tokA0")
    tok_wait(True, 0, xl, 0, 0)
    send_tok(xl, 0, 0, True, 2)
    send_tok(x, 0, 1, True, 3)
    tok_wait(False, 0, xr, 1, 0)
    send_tok(xr, 1, 0, False, 2)
    send_tok(x, 1, 1, False, 3)
    ph("gu_near")
    gu.near()
    ph("own_mate")
    to_mate(0, x, 0)
    to_mate(1, x, 1)

    tails = []
    for h in range(2):
        f = rr[x, c, h, HALF - 8:HALF, :][:, 0:1]
        for r in (6, 7):
            for q in range(8):
                ch, col = q // 4, (q % 4) * 256
                v = tok[x, c, ch, (h + 1) * HALF - 16:(h + 1) * HALF, col:col + 256].astype(F32)
                tails.append(v[r + 8:r + 9] * f[r:r + 1])
    hal[tp] = jnp.concatenate(tails, axis=0).astype(BF16)
    for k in range(1, 8):
        cp = rcopy(hal.at[tp], hal.at[tp], h_s.at[k], h_r.at[8 - k], (tp + k) % 8)
        cp.start()
        drains.append(cp)

    ph("gu_c0")
    gu.cross(0)
    ph("gu_far")
    gu.far()
    ld_dw.wait()
    gd.start()
    ph("gu_c1")
    gu.cross(1)
    ph("gu_c2")
    gu.cross(2)
    ph("gu_c3")
    gu.cross(3)
    ph("gd_near")
    gd.near()
    ph("gu_last")
    for i in range(4):
        gu.last(i)
    ph("tokA1")
    tok_wait(True, 3, xl, 0, 1)
    send_tok(xl, 0, 1, True, 4)
    send_tok(x, 1, 1, True, 5)
    tok_wait(False, 3, xr, 1, 1)
    send_tok(xr, 1, 1, False, 4)
    send_tok(x, 0, 1, False, 5)
    to_mate(2, xl, 0)
    to_mate(3, xr, 1)

    ph("xexp")
    for k in range(1, 8):
        src = (tp + k) % 8
        rcopy(hal.at[src], hal.at[src], h_s.at[k], h_r.at[k], mate).wait_recv()
    hv = hal[...].reshape(256, 256).astype(F32)
    rid = lax.broadcasted_iota(jnp.int32, (256, 256), 0) % 8
    for q in range(8):
        xexp[:, q * 256:(q + 1) * 256] = jnp.where(rid == q, hv, 0.0).astype(BF16)

    ph("gd_c0")
    gd.cross(0)
    ph("hu")

    @pl.loop(0, 6)
    def _(i):
        w = ug[:, :, :, pl.ds(pl.multiple_of(i * 256, 256), 128)].reshape(D, 128)
        r = jnp.dot(xexp[...], w, preferred_element_type=F32)
        r = jnp.sum(r.reshape(32, 8, 128), axis=1)
        cols = pl.ds(pl.multiple_of(i * 128, 128), 128)
        hu[0, 0:2, cols] = jnp.zeros((2, 128), F32)
        for q in range(15):
            hu[q + 1, 0:2, cols] = r[2 * q:2 * q + 2]

    row8 = lax.broadcasted_iota(jnp.int32, (8, 128), 0)

    def hidden(xs, hs, cc, to):
        unit = [(xs[k] * 2 + cc) * 2 + hs[k] for k in range(2)]
        a = [[tok[xs[k], cc, ch, hs[k] * HALF:(hs[k] + 1) * HALF, :] for ch in range(2)]
             for k in range(2)]
        a = jnp.concatenate([jnp.concatenate(v, axis=1) for v in a], axis=0)

        def act(i, u, g):
            cols = pl.ds(i * 128, 128)
            taps = [cw[k:k + 1, cols] for k in range(4)]
            for k in range(2):
                f = rr[xs[k], cc, hs[k]]
                uk, gk = u[k * HALF:(k + 1) * HALF] * f, g[k * HALF:(k + 1) * HALF] * f
                before = hu[unit[k], :, cols]
                h0, h1 = before[0:1], before[1:2]
                u1, u2 = pltpu.roll(uk, 1, 0), pltpu.roll(uk, 2, 0)
                f1 = jnp.where(row8 == 0, h1, u1[:8])
                f2 = jnp.where(row8 == 0, h0, jnp.where(row8 == 1, h1, u2[:8]))
                u1 = jnp.concatenate([f1, u1[8:]], axis=0)
                u2 = jnp.concatenate([f2, u2[8:]], axis=0)
                s = taps[3] + taps[0] * u2 + taps[1] * u1 + taps[2] * uk
                hid[to, pl.ds(k * HALF, HALF), cols] = gated_gelu(s, gk).astype(BF16)

        for i, width in ((0, 512), (2, 512), (4, 384)):
            w = ug[:, :, :, pl.ds(i * 256, width)].reshape(D, width)
            r = jnp.dot(a, w, preferred_element_type=F32)
            act(i, r[:, :128], r[:, 128:256])
            if width == 512:
                act(i + 1, r[:, 256:384], r[:, 384:])
            else:
                act(i + 1, r[:, 256:384], pltpu.roll(r[:, 256:384], 64, 1))

    def down(frm, xs, hs, cls):
        @pl.loop(0, 4)
        def _(n):
            w = jnp.concatenate([dwn[n, k] for k in range(4)], axis=1)
            r = jnp.dot(hid[frm], w, preferred_element_type=F32).astype(BF16)
            cols = pl.ds(pl.multiple_of(n * 512, 512), 512)
            for k in range(2):
                pbuf[cls, xs[k], hs[k], :, cols] = r[k * HALF:(k + 1) * HALF]

        @pl.when(cls == 0)
        def _():
            for k in range(2):
                rcopy(pbuf.at[0, xs[k], hs[k]], precv.at[xs[k], hs[k]], p_s.at[xs[k], hs[k]],
                      p_r.at[xs[k], hs[k]], mate).start()

    def core_of(cls):
        return (1 - c) * (1 - cls) + c * cls

    def group(xs, hs, slot=None, up=True, dn=True):
        @pl.loop(0, 2)
        def _(cls):
            to = cls if slot is None else slot + cls
            if up:
                hidden(xs, hs, core_of(cls), to)
            if dn:
                down(to, xs, hs, cls)

    ph("gd_far")
    gd.far()
    ph("gd_c1")
    gd.cross(1)
    ph("mate_own")
    mate_wait(0, x, 0)
    mate_wait(1, x, 1)
    ph("h_own")
    group((x, x), (0, 1), 2, dn=False)
    ph("gd_c23")
    gd.cross(2)
    gd.cross(3)

    ph("tok_opp")
    tok_wait(True, 2, xo, 0, 0)
    tok_wait(True, 4, xo, 0, 1)
    to_mate(4, xo, 0)
    tok_wait(False, 2, xo, 1, 0)
    tok_wait(False, 4, xo, 1, 1)
    to_mate(5, xo, 1)
    ph("mate_opp")
    mate_wait(4, xo, 0)
    mate_wait(5, xo, 1)
    ph("h_opp")
    group((xo, xo), (0, 1), 0, dn=False)
    ph("gd_last")
    for i in range(4):
        gd.last(i)
    mate_wait(2, xl, 0)
    mate_wait(3, xr, 1)

    def joined(xx, h, extra=None):
        rcopy(pbuf.at[0, xx, h], precv.at[xx, h], p_s.at[xx, h], p_r.at[xx, h], mate).wait_recv()

        @pl.loop(0, HALF // 16)
        def _(r):
            rr = pl.ds(pl.multiple_of(r * 16, 16), 16)
            v = pbuf[1, xx, h, rr, :].astype(F32) + precv[xx, h, rr, :].astype(F32)
            if extra is not None:
                v = v + extra[rr, :].astype(F32)
            pbuf[1, xx, h, rr, :] = v.astype(BF16)

    def send_sum(xx, h, to_right, dst, k):
        side = 0 if to_right else 1
        cp = rcopy(pbuf.at[1, xx, h], dst, x_s.at[side, k], x_r.at[side, k],
                   (xr if to_right else xl) * 2 + c)
        cp.start()
        drains.append(cp)

    def wait_sum(from_left, dst, k):
        side = 0 if from_left else 1
        rcopy(dst, dst, x_s.at[side, k], x_r.at[side, k], mate).wait_recv()

    ph("d_opp")
    group((xo, xo), (0, 1), 0, up=False)
    ph("j_opp")
    joined(xo, 0)
    send_sum(xo, 0, True, xfwd.at[0], 0)
    joined(xo, 1)
    send_sum(xo, 1, False, xfwd.at[1], 0)
    ph("g_near1")
    group((xr, xl), (1, 0))
    ph("j_near1")
    joined(xr, 1)
    send_sum(xr, 1, True, xfin.at[0, 1], 1)
    joined(xl, 0)
    send_sum(xl, 0, False, xfin.at[1, 0], 1)

    ph("tok_near2")
    tok_wait(True, 1, xl, 1, 0)
    tok_wait(True, 5, xl, 1, 1)
    to_mate(6, xl, 1)
    tok_wait(False, 1, xr, 0, 0)
    tok_wait(False, 5, xr, 0, 1)
    to_mate(7, xr, 0)
    mate_wait(6, xl, 1)
    mate_wait(7, xr, 0)
    ph("g_near2")
    group((xr, xl), (0, 1))
    ph("j_near2")
    wait_sum(True, xfwd.at[0], 0)
    joined(xr, 0, xfwd.at[0])
    send_sum(xr, 0, True, xfin.at[0, 0], 2)
    ph("j_near2b")
    wait_sum(False, xfwd.at[1], 0)
    joined(xl, 1, xfwd.at[1])
    send_sum(xl, 1, False, xfin.at[1, 1], 2)

    ph("d_own")
    group((x, x), (0, 1), 2, up=False)
    ph("base")
    outs = []
    for h in range(2):
        rcopy(pbuf.at[0, x, h], precv.at[x, h], p_s.at[x, h], p_r.at[x, h], mate).wait_recv()

        @pl.loop(0, HALF // 16)
        def _(r):
            row = pl.ds(pl.multiple_of(r * 16, 16), 16)
            at = pl.ds(pl.multiple_of(h * HALF + r * 16, 16), 16)
            for ch in range(2):
                cols = pl.ds(ch * CH, CH)
                v = tok[x, c, ch, at, :].astype(F32) + pbuf[1, x, h, row, cols].astype(F32)
                base[at, cols] = v + precv[x, h, row, cols].astype(F32)

        cp = pltpu.make_async_copy(base.at[pl.ds(h * HALF, HALF)], out.at[pl.ds(h * HALF, HALF)],
                                   lsem.at[5 + h])
        cp.start()
        outs.append(cp)
    for cp in outs:
        cp.wait()

    ph("fin_w1")
    wait_sum(True, xfin.at[0, 1], 1)
    wait_sum(False, xfin.at[1, 0], 1)
    ph("fin_w2")
    wait_sum(True, xfin.at[0, 0], 2)
    wait_sum(False, xfin.at[1, 1], 2)

    ph("drain")
    @pl.when(c != half)
    def _():
        for cp in overs:
            cp.wait_send()

    for cp in drains:
        cp.wait_send()
    gw.drain()
    gv.drain()
    gu.drain()
    gd.drain()
    for xx in range(4):
        for h in range(2):
            rcopy(pbuf.at[0, xx, h], precv.at[xx, h], p_s.at[xx, h], p_r.at[xx, h],
                  mate).wait_send()
    ph("")


def body(mixed, residual, mix_weight, norm_gain, up_weight, gate_weight, conv_weight, conv_bias,
         down_weight):
    any_ = pl.BlockSpec(memory_space=pl.ANY)
    vm = pl.BlockSpec(memory_space=pltpu.VMEM)
    dma = pltpu.SemaphoreType.DMA
    part, sums = pl.pallas_call(
        kernel,
        out_shape=(jax.ShapeDtypeStruct((TOK, D), F32),
                   jax.ShapeDtypeStruct((2, 2, HALF, D), BF16)),
        in_specs=[any_, any_, any_, vm, any_, any_, vm, vm, any_],
        out_specs=(any_, any_),
        scratch_shapes=[
            pltpu.VMEM((2, 4, 4, 128, CH), BF16),
            pltpu.VMEM((4, 4, 128, UG), BF16),
            pltpu.VMEM((4, 4, HID, 128), BF16),
            pltpu.VMEM((2, 688, 128), BF16),
            pltpu.VMEM((8, HID), F32),
            pltpu.VMEM((4, 2, 2, TOK, CH), BF16),
            pltpu.VMEM((4, 2, 2, HALF, 128), F32),
            pltpu.VMEM((TOK, D), BF16),
            pltpu.VMEM((TOK, D), BF16),
            pltpu.VMEM((8, 32, 256), BF16),
            pltpu.VMEM((256, D), BF16),
            pltpu.VMEM((16, 8, HID), F32),
            pltpu.VMEM((4, TOK, HID), BF16),
            pltpu.VMEM((2, 4, 2, HALF, D), BF16),
            pltpu.VMEM((4, 2, HALF, D), BF16),
            pltpu.VMEM((2, HALF, D), BF16),
            pltpu.VMEM((TOK, D), F32),
            dma((7,)), dma((2, 4)), dma((2, 4)),
            dma((4, 16)), dma((4, 16)),
            dma((2, 16)), dma((2, 16)),
            dma((2, 6)), dma((2, 6)),
            dma((8,)), dma((8,)), dma((8,)), dma((8,)),
            dma((8,)), dma((8,)),
            dma((4, 2)), dma((4, 2)),
            dma((2, 3)), dma((2, 3)),
        ],
        compiler_params=pltpu.CompilerParams(
            collective_id=0, has_side_effects=True, vmem_limit_bytes=67_043_328),
    )(mixed, residual, mix_weight, norm_gain[None], up_weight.T, gate_weight.T, conv_weight, conv_bias,
      down_weight)
    sums = sums.reshape(2, TOK, D).astype(F32)
    return (part + sums[0] + sums[1]).astype(BF16)


def solution(mesh):
    rows = P(("fs", "tp"), None)
    in_specs = (rows, rows, rows, P(), P("fs", "tp"), P("fs", "tp"), P(None, "tp"), P("tp"),
                P("tp", "fs"))
    return jax.shard_map(body, mesh=mesh, in_specs=in_specs, out_specs=rows, check_vma=False)
```

time: 189 us -> 162 us (0.86)
  Pallas kernels: 179 us -> 157 us
  local copies, waits for them, and re-layouts: 9.48 us -> 2.87 us
    pallas_call x1, Pallas kernels: 179 us -> 157 us  [body(): pl.pallas_call(kernel, out_shape=(jax.ShapeDtypeStruct((TOK, D), F32), ja...]
    unnamed x13 -> x2, local copies, waits for them, and re-layouts: 4.15 us -> 0.01 us
    convert_element_type x0 -> x1, other arithmetic: none -> 2.18 us  [body(): return (part + sums[0] + sums[1]).astype(BF16)]
where the time goes in v2:
time: 162 us
  Pallas kernels  157 us (97%)
  local copies, waits for them, and re-layouts  2.87 us (2%)
  other arithmetic  2.18 us (1%)
    pallas_call x1, Pallas kernels, body(): pl.pallas_call(kernel, out_shape=(jax.ShapeDtypeStruct((TOK, D), F32), ja...  157 us

profile of v2, /device:TPU:1, one launch (start us, length us, event | category | flops | bytes accessed | tf_op | source)
XLA Modules:
  0.0 161.9 jit_solution(2832618320498215954)
XLA Ops:
  0.0 156.8 %shard_map.91 = (f32[384,2048]{1,0:T(8,128)}, bf16[2,2,192,2048]{3,2,1,0:T(8,128)(2,1)}) custom-call(bf16[384,2048]{1,0:T(8,128)(2,1)} %mixed.1, bf16[384,2048]{1,0:T(8,128)(2,1)} %resid.1, bf16[16,2048]{1,0:T(8,128)(2,1)} %wm_in.1, f32[1,2048]{1,0:T(1,128)} %bitcast.13, bf16[688,128]{1,0:T(8,128)(2,1)} %bitcast.11, bf16[688,128]{1,0:T(8,128)(2,1)} %bitcast.12, ...), custom_call_target="tpu_custom_call" | custom-call | tf_op jit(solution)/shard_map/pallas_call | solution.py:625
  156.8 0.0 copy-start
  156.8 2.9 %fusion.1 = (f32[1,2,192,2048]{3,2,1,0:T(8,128)S(1)}, f32[1,2,192,2048]{3,2,1,0:T(8,128)S(1)}) fusion(bf16[2,2,192,2048]{3,2,1,0:T(8,128)(2,1)} %get-tuple-element.8), kind=kLoop, calls=%fused_computation.3 | loop fusion | bytes 12582912 | tf_op jit(solution)/shard_map/slice | solution.py:663
  159.7 0.0 copy-done
  159.7 2.2 %fusion = bf16[384,2048]{1,0:T(8,128)(2,1)} fusion(f32[1,2,192,2048]{3,2,1,0:T(8,128)S(1)} %get-tuple-element.10, f32[384,2048]{1,0:T(8,128)S(1)} %copy-done, f32[1,2,192,2048]{3,2,1,0:T(8,128)S(1)} %get-tuple-element.9), kind=kLoop, calls=%fused_computation.1 | loop fusion | flops 2359296 | bytes 11010048 | tf_op jit(solution)/shard_map/convert_element_type | solution.py:663
Async XLA Ops:
  156.8 2.9 %copy-start = (f32[384,2048]{1,0:T(8,128)S(1)}, f32[384,2048]{1,0:T(8,128)}, u32[]{:S(2)}) copy-start(f32[384,2048]{1,0:T(8,128)} %get-tuple-element.7) | copy-start | bytes 9437188

commit v3 on v2

--- a/solution.py
+++ b/solution.py
@@ -92,13 +92,15 @@
         self.send(2, self.view(-1, 0, 0, s), (1, 0))
         self.both(1)
         self.wait(1, self.view(1, 0))
-        self.send(3, self.view(1, 0, s, self.rows - s), (-1, 0))
+        if s < self.rows:
+            self.send(3, self.view(1, 0, s, self.rows - s), (-1, 0))
         self.both(2)
 
     def far(self):
         s = self.split
         self.wait(2, self.view(2, 0, 0, s))
-        self.wait(3, self.view(2, 0, s, self.rows - s))
+        if s < self.rows:
+            self.wait(3, self.view(2, 0, s, self.rows - s))
         self.both(3)
 
     def cross(self, i):
@@ -118,10 +120,10 @@
             c.wait_send()
 
 
-def kernel(mixed, resid, wm_in, gain, up_in, gate_in, cw_in, cb_in, dw_in, out, xfin,
-           wm, ug, dwn, upt, cw, tok, rr, mx, rs, hal, xexp, hu, hid, pbuf, precv, xfwd, base,
+def kernel(mixed, resid, wm_in, gain, up_in, gate_in, cw_in, cb_in, dw_in, out, sum_l, sum_r,
+           wm, ug, dwn, upt, cw, tok, rr, mx, rs, hal, hu, hid, pbuf, precv, xfwd, base,
            lsem, wx_s, wx_r, g_s, g_r, d_s, d_r, t_s, t_r, td_s, td_r, rd_s, rd_r, h_s, h_r,
-           p_s, p_r, x_s, x_r):
+           p_s, p_r, x_s, x_r, xw_s, xw_r, xd_s, xd_r):
     fs, tp = lax.axis_index("fs"), lax.axis_index("tp")
     z, y, x, c = fs // 4, fs % 4, tp // 2, tp % 2
     xr, xl, xo = (x + 1) % 4, (x + 3) % 4, (x + 2) % 4
@@ -140,6 +142,10 @@
     ld_dw = pltpu.make_async_copy(dw_in, dwn.at[z, y, pl.ds(0, 688)], lsem.at[1])
     ld_mx = pltpu.make_async_copy(mixed, mx, lsem.at[2])
     ld_rs = pltpu.make_async_copy(resid, rs, lsem.at[3])
+    row16 = pl.multiple_of(tp * 16, 16)
+    ld_own = pltpu.make_async_copy(wm_in.at[:, pl.ds(CH, CH)], wm.at[1, z, y, pl.ds(row16, 16)],
+                                   lsem.at[7])
+    ld_own.start()
     ld_up.start()
     ld_gate.start()
     ld_mx.start()
@@ -157,77 +163,75 @@
 
     ph("wx")
     half = tp // 4
-    row16 = pl.multiple_of(tp * 16, 16)
     slot = tp % 4
-    stays, overs = [], []
-    for ch in range(2):
-        src = wm_in.at[:, pl.ds(ch * CH, CH)]
-        dst = wm.at[ch, z, y, pl.ds(row16, 16)]
-        for k in range(1, 4):
-            cp = rcopy(src, dst, wx_s.at[ch, k], wx_r.at[ch, slot], ((x + k) % 4) * 2 + half)
-            cp.start()
-            drains.append(cp)
-        stays.append(pltpu.make_async_copy(src, dst, wx_r.at[ch, slot]))
-        overs.append(rcopy(src, dst, wx_s.at[ch, 0], wx_r.at[ch, slot], mate))
+    src = wm_in.at[:, pl.ds(0, CH)]
+    dst = wm.at[0, z, y, pl.ds(row16, 16)]
+    for k in range(1, 4):
+        cp = rcopy(src, dst, wx_s.at[k], wx_r.at[slot], ((x + k) % 4) * 2 + half)
+        cp.start()
+        drains.append(cp)
+    stay = pltpu.make_async_copy(src, dst, wx_r.at[slot])
+    over = rcopy(src, dst, wx_s.at[0], wx_r.at[slot], mate)
 
     @pl.when(c == half)
     def _():
-        for cp in stays:
-            cp.start()
+        stay.start()
 
     @pl.when(c != half)
     def _():
-        for cp in overs:
-            cp.start()
+        over.start()
 
     lo = pl.multiple_of(c * 64, 64)
     other = pl.multiple_of(64 - lo, 64)
-    gws = [Gather(wm.at[ch], lo, 64, 32, c, fs, tp, g_s.at[ch], g_r.at[ch]) for ch in range(2)]
-    gw, gv = gws
+    gw = Gather(wm.at[0], lo, 64, 32, c, fs, tp, g_s.at[0], g_r.at[0])
+    gv = Gather(wm.at[1], row16, 16, 16, c, fs, tp, g_s.at[1], g_r.at[1])
     gu = Gather(ug, 0, 128, 64, c, fs, tp, g_s.at[2], g_r.at[2])
     gd = Gather(dwn, 0, 688, 352, 1 - c, fs, tp, g_s.at[3], g_r.at[3])
 
-    def share(ch, k, dp, ds):
-        blk = gws[ch].view(dp, ds)
-        cp = rcopy(blk, blk, d_s.at[ch, k], d_r.at[ch, k], mate)
-        cp.start()
-        drains.append(cp)
-
-    def shared(ch):
-        for k in range(16):
-            blk = wm.at[ch, k // 4, k % 4, pl.ds(other, 64)]
-            rcopy(blk, blk, d_s.at[ch, k], d_r.at[ch, k], mate).wait_recv()
-
-    def w_start(ch):
-        for k in range(4):
-            row = pl.multiple_of(lo + k * 16, 16)
-            blk = wm.at[ch, z, y, pl.ds(row, 16)]
-            rcopy(blk, blk, wx_s.at[ch, 0], wx_r.at[ch, k], mate).wait_recv()
-        gws[ch].start()
-        share(ch, 0, 0, 0)
-
-    def w_near(ch):
-        gws[ch].near()
-        share(ch, 1, -1, 0)
-        share(ch, 2, 1, 0)
-
-    def w_far(ch):
-        gws[ch].far()
-        share(ch, 3, 2, 0)
-
-    def w_cross(ch, i):
-        gws[ch].cross(i)
-        share(ch, 4 + 2 * i, Gather.REL[i], -1)
-        share(ch, 5 + 2 * i, Gather.REL[i], 1)
-
-    def w_last(ch):
-        for i in range(4):
-            gws[ch].last(i)
-            share(ch, 12 + i, Gather.REL[i], 2)
-
+    def share(k, dp, ds):
+        blk = gw.view(dp, ds)
+        cp = rcopy(blk, blk, d_s.at[k], d_r.at[k], mate)
+        cp.start()
+        drains.append(cp)
+
+    def w_cross(i):
+        gw.cross(i)
+        share(4 + 2 * i, Gather.REL[i], -1)
+        share(5 + 2 * i, Gather.REL[i], 1)
+
+    def w_rows(xsrc, core, z0=0, nz=4):
+        return wm.at[1, pl.ds(z0, nz), :, pl.ds(pl.multiple_of((xsrc * 2 + core) * 16, 16), 16)]
+
+    def line_send(to_right, k, xsrc, z0, nz):
+        side, blk = 0 if to_right else 1, w_rows(xsrc, c, z0, nz)
+        cp = rcopy(blk, blk, xw_s.at[side, k], xw_r.at[side, k], (xr if to_right else xl) * 2 + c)
+        cp.start()
+        drains.append(cp)
+
+    def line_wait(from_left, k, xsrc, z0, nz):
+        side, blk = 0 if from_left else 1, w_rows(xsrc, c, z0, nz)
+        rcopy(blk, blk, xw_s.at[side, k], xw_r.at[side, k], mate).wait_recv()
+
+    def line_share(k, xsrc):
+        blk = w_rows(xsrc, c)
+        cp = rcopy(blk, blk, xd_s.at[k], xd_r.at[k], mate)
+        cp.start()
+        drains.append(cp)
+
+    ph("v_start")
+    ld_own.wait()
+    gv.start()
+    gv.near()
     ph("w_start")
-    w_start(0)
-    w_start(1)
+    for k in range(4):
+        row = pl.multiple_of(lo + k * 16, 16)
+        blk = wm.at[0, z, y, pl.ds(row, 16)]
+        rcopy(blk, blk, wx_s.at[0], wx_r.at[k], mate).wait_recv()
+    gw.start()
+    share(0, 0, 0)
+    ph("v_far")
+    gv.cross(0)
+    gv.far()
 
     ph("prep")
     zero_rows = jnp.zeros((HID - 688, 128), BF16)
@@ -280,11 +284,13 @@
         m = jnp.sum(acc, axis=-1, keepdims=True) * (1.0 / D)
         rr[xsrc, c, h] = jnp.broadcast_to(lax.rsqrt(m + NORM_EPS), (HALF, 128))
 
-    def to_mate(k, xsrc, h):
-        blk = tok.at[xsrc, c, :, pl.ds(h * HALF, HALF)]
-        cp = rcopy(blk, blk, td_s.at[k], td_r.at[k], mate)
-        cp.start()
-        drains.append(cp)
+    def pass_on(k, xsrc, h, ch):
+        blk = tok.at[xsrc, c, ch, pl.ds(h * HALF, HALF)]
+        cp = rcopy(blk, blk, td_s.at[k, ch], td_r.at[k, ch], mate)
+        cp.start()
+        drains.append(cp)
+
+    def pass_factor(k, xsrc, h):
         factor(xsrc, h)
         blk = rr.at[xsrc, c, h]
         cp = rcopy(blk, blk, rd_s.at[k], rd_r.at[k], mate)
@@ -292,69 +298,83 @@
         drains.append(cp)
 
     def mate_wait(k, xsrc, h):
-        blk = tok.at[xsrc, 1 - c, :, pl.ds(h * HALF, HALF)]
-        rcopy(blk, blk, td_s.at[k], td_r.at[k], mate).wait_recv()
+        for ch in range(2):
+            blk = tok.at[xsrc, 1 - c, ch, pl.ds(h * HALF, HALF)]
+            rcopy(blk, blk, td_s.at[k, ch], td_r.at[k, ch], mate).wait_recv()
         blk = rr.at[xsrc, 1 - c, h]
         rcopy(blk, blk, rd_s.at[k], rd_r.at[k], mate).wait_recv()
 
-    ph("w0_near")
-    w_near(0)
-    ph("w0_c0")
-    w_cross(0, 0)
-    ph("w0_far")
-    w_far(0)
-    ph("w1_near")
-    w_near(1)
-    ph("w0_c1")
-    w_cross(0, 1)
-    ph("w0_c2")
-    w_cross(0, 2)
-    ph("w1_c0")
-    w_cross(1, 0)
-    ph("w1_far")
-    w_far(1)
-    ph("w0_c3")
-    w_cross(0, 3)
-    ph("w1_c1")
-    w_cross(1, 1)
-    ph("w0_last")
-    w_last(0)
-    ph("w0_shared")
-    shared(0)
+    ph("w_near")
+    gw.near()
+    share(1, -1, 0)
+    share(2, 1, 0)
+    ph("v_c12")
+    gv.cross(1)
+    gv.cross(2)
+    ph("w_c0")
+    w_cross(0)
+    ph("v_last")
+    gv.cross(3)
+    for i in range(4):
+        gv.last(i)
+    line_send(True, 0, x, 0, 4)
+    line_send(False, 0, x, 0, 4)
+    line_share(0, x)
+    ph("w_far")
+    gw.far()
+    share(3, 2, 0)
+    ph("w_c1")
+    w_cross(1)
+    ph("w_c2")
+    w_cross(2)
+    ph("w_c3")
+    w_cross(3)
+    gu.start()
+    ph("w_last")
+    for i in range(4):
+        gw.last(i)
+        share(12 + i, Gather.REL[i], 2)
+    ph("line_fwd")
+    line_wait(True, 0, xl, 0, 4)
+    line_send(True, 1, xl, 0, 2)
+    line_share(1, xl)
+    line_wait(False, 0, xr, 0, 4)
+    line_send(False, 1, xr, 2, 2)
+    line_share(2, xr)
+    ph("w_shared")
+    for k in range(16):
+        blk = wm.at[0, k // 4, k % 4, pl.ds(other, 64)]
+        rcopy(blk, blk, d_s.at[k], d_r.at[k], mate).wait_recv()
     ld_mx.wait()
     ld_rs.wait()
     ph("mix0")
     mix(0, 0)
-    ph("w1_c2")
-    w_cross(1, 2)
-    ph("mix1")
     mix(0, 1)
     send_tok(x, 0, 0, True, 0)
     send_tok(x, 1, 0, False, 0)
-    send_tok(x, 1, 0, True, 1)
-    send_tok(x, 0, 0, False, 1)
-    ph("w1_c3")
-    w_cross(1, 3)
-    gu.start()
-    ph("w1_last")
-    w_last(1)
-    ph("w1_shared")
-    shared(1)
-    ph("mix2")
+    pass_on(0, x, 0, 0)
+    pass_on(1, x, 1, 0)
+    ph("gu_near")
+    gu.near()
+    ph("line_far")
+    line_wait(True, 1, xo, 0, 2)
+    line_wait(False, 1, xo, 2, 2)
+    line_share(3, xo)
+    for k, xsrc in enumerate((x, xl, xr, xo)):
+        blk = w_rows(xsrc, 1 - c)
+        rcopy(blk, blk, xd_s.at[k], xd_r.at[k], mate).wait_recv()
+    ph("mix1")
     mix(1, 0)
     mix(1, 1)
-    ph("tokA0")
-    tok_wait(True, 0, xl, 0, 0)
-    send_tok(xl, 0, 0, True, 2)
-    send_tok(x, 0, 1, True, 3)
-    tok_wait(False, 0, xr, 1, 0)
-    send_tok(xr, 1, 0, False, 2)
-    send_tok(x, 1, 1, False, 3)
-    ph("gu_near")
-    gu.near()
+    send_tok(x, 0, 1, True, 1)
+    send_tok(x, 1, 1, False, 1)
+    pass_on(0, x, 0, 1)
+    pass_on(1, x, 1, 1)
+    ph("gu_c0")
+    gu.cross(0)
     ph("own_mate")
-    to_mate(0, x, 0)
-    to_mate(1, x, 1)
+    pass_factor(0, x, 0)
+    pass_factor(1, x, 1)
 
     tails = []
     for h in range(2):
@@ -370,32 +390,41 @@
         cp.start()
         drains.append(cp)
 
-    ph("gu_c0")
-    gu.cross(0)
     ph("gu_far")
     gu.far()
-    ld_dw.wait()
-    gd.start()
+    ph("tokA0")
+    tok_wait(True, 0, xl, 0, 0)
+    send_tok(xl, 0, 0, True, 2)
+    pass_on(2, xl, 0, 0)
+    tok_wait(False, 0, xr, 1, 0)
+    send_tok(xr, 1, 0, False, 2)
+    pass_on(3, xr, 1, 0)
     ph("gu_c1")
     gu.cross(1)
     ph("gu_c2")
     gu.cross(2)
     ph("gu_c3")
     gu.cross(3)
-    ph("gd_near")
-    gd.near()
+    ld_dw.wait()
+    gd.start()
+    ph("tokA1")
+    tok_wait(True, 1, xl, 0, 1)
+    send_tok(xl, 0, 1, True, 3)
+    send_tok(x, 1, 0, True, 4)
+    send_tok(x, 1, 1, True, 5)
+    pass_on(2, xl, 0, 1)
+    tok_wait(False, 1, xr, 1, 1)
+    send_tok(xr, 1, 1, False, 3)
+    send_tok(x, 0, 0, False, 4)
+    send_tok(x, 0, 1, False, 5)
+    pass_on(3, xr, 1, 1)
+    pass_factor(2, xl, 0)
+    pass_factor(3, xr, 1)
     ph("gu_last")
     for i in range(4):
         gu.last(i)
-    ph("tokA1")
-    tok_wait(True, 3, xl, 0, 1)
-    send_tok(xl, 0, 1, True, 4)
-    send_tok(x, 1, 1, True, 5)
-    tok_wait(False, 3, xr, 1, 1)
-    send_tok(xr, 1, 1, False, 4)
-    send_tok(x, 0, 1, False, 5)
-    to_mate(2, xl, 0)
-    to_mate(3, xr, 1)
+    ph("gd_near")
+    gd.near()
 
     ph("xexp")
     for k in range(1, 8):
@@ -404,7 +433,7 @@
     hv = hal[...].reshape(256, 256).astype(F32)
     rid = lax.broadcasted_iota(jnp.int32, (256, 256), 0) % 8
     for q in range(8):
-        xexp[:, q * 256:(q + 1) * 256] = jnp.where(rid == q, hv, 0.0).astype(BF16)
+        mx[0:256, q * 256:(q + 1) * 256] = jnp.where(rid == q, hv, 0.0).astype(BF16)
 
     ph("gd_c0")
     gd.cross(0)
@@ -413,7 +442,7 @@
     @pl.loop(0, 6)
     def _(i):
         w = ug[:, :, :, pl.ds(pl.multiple_of(i * 256, 256), 128)].reshape(D, 128)
-        r = jnp.dot(xexp[...], w, preferred_element_type=F32)
+        r = jnp.dot(mx[0:256, :], w, preferred_element_type=F32)
         r = jnp.sum(r.reshape(32, 8, 128), axis=1)
         cols = pl.ds(pl.multiple_of(i * 128, 128), 128)
         hu[0, 0:2, cols] = jnp.zeros((2, 128), F32)
@@ -480,37 +509,6 @@
             if dn:
                 down(to, xs, hs, cls)
 
-    ph("gd_far")
-    gd.far()
-    ph("gd_c1")
-    gd.cross(1)
-    ph("mate_own")
-    mate_wait(0, x, 0)
-    mate_wait(1, x, 1)
-    ph("h_own")
-    group((x, x), (0, 1), 2, dn=False)
-    ph("gd_c23")
-    gd.cross(2)
-    gd.cross(3)
-
-    ph("tok_opp")
-    tok_wait(True, 2, xo, 0, 0)
-    tok_wait(True, 4, xo, 0, 1)
-    to_mate(4, xo, 0)
-    tok_wait(False, 2, xo, 1, 0)
-    tok_wait(False, 4, xo, 1, 1)
-    to_mate(5, xo, 1)
-    ph("mate_opp")
-    mate_wait(4, xo, 0)
-    mate_wait(5, xo, 1)
-    ph("h_opp")
-    group((xo, xo), (0, 1), 0, dn=False)
-    ph("gd_last")
-    for i in range(4):
-        gd.last(i)
-    mate_wait(2, xl, 0)
-    mate_wait(3, xr, 1)
-
     def joined(xx, h, extra=None):
         rcopy(pbuf.at[0, xx, h], precv.at[xx, h], p_s.at[xx, h], p_r.at[xx, h], mate).wait_recv()
 
@@ -533,6 +531,43 @@
         side = 0 if from_left else 1
         rcopy(dst, dst, x_s.at[side, k], x_r.at[side, k], mate).wait_recv()
 
+    ph("gd_far")
+    gd.far()
+    ph("mate_own")
+    mate_wait(0, x, 0)
+    mate_wait(1, x, 1)
+    ph("h_own0")
+    hidden((x, x), (0, 1), core_of(0), 2)
+    ph("gd_c12")
+    gd.cross(1)
+    gd.cross(2)
+    ph("h_own1")
+    hidden((x, x), (0, 1), core_of(1), 3)
+    ph("gd_c3")
+    gd.cross(3)
+
+    ph("tok_opp")
+    tok_wait(True, 2, xo, 0, 0)
+    pass_on(4, xo, 0, 0)
+    tok_wait(False, 2, xo, 1, 0)
+    pass_on(5, xo, 1, 0)
+    tok_wait(True, 3, xo, 0, 1)
+    pass_on(4, xo, 0, 1)
+    pass_factor(4, xo, 0)
+    tok_wait(False, 3, xo, 1, 1)
+    pass_on(5, xo, 1, 1)
+    pass_factor(5, xo, 1)
+    ph("h_opp1")
+    hidden((xo, xo), (0, 1), core_of(1), 1)
+    ph("mate_opp")
+    mate_wait(4, xo, 0)
+    mate_wait(5, xo, 1)
+    ph("h_opp0")
+    hidden((xo, xo), (0, 1), core_of(0), 0)
+    ph("gd_last")
+    for i in range(4):
+        gd.last(i)
+
     ph("d_opp")
     group((xo, xo), (0, 1), 0, up=False)
     ph("j_opp")
@@ -540,21 +575,28 @@
     send_sum(xo, 0, True, xfwd.at[0], 0)
     joined(xo, 1)
     send_sum(xo, 1, False, xfwd.at[1], 0)
+    ph("mate_near1")
+    mate_wait(2, xl, 0)
+    mate_wait(3, xr, 1)
     ph("g_near1")
     group((xr, xl), (1, 0))
     ph("j_near1")
     joined(xr, 1)
-    send_sum(xr, 1, True, xfin.at[0, 1], 1)
+    send_sum(xr, 1, True, sum_l.at[pl.ds(HALF, HALF)], 1)
     joined(xl, 0)
-    send_sum(xl, 0, False, xfin.at[1, 0], 1)
+    send_sum(xl, 0, False, sum_r.at[pl.ds(0, HALF)], 1)
 
     ph("tok_near2")
-    tok_wait(True, 1, xl, 1, 0)
+    tok_wait(True, 4, xl, 1, 0)
+    pass_on(6, xl, 1, 0)
+    tok_wait(False, 4, xr, 0, 0)
+    pass_on(7, xr, 0, 0)
     tok_wait(True, 5, xl, 1, 1)
-    to_mate(6, xl, 1)
-    tok_wait(False, 1, xr, 0, 0)
+    pass_on(6, xl, 1, 1)
+    pass_factor(6, xl, 1)
     tok_wait(False, 5, xr, 0, 1)
-    to_mate(7, xr, 0)
+    pass_on(7, xr, 0, 1)
+    pass_factor(7, xr, 0)
     mate_wait(6, xl, 1)
     mate_wait(7, xr, 0)
     ph("g_near2")
@@ -562,11 +604,11 @@
     ph("j_near2")
     wait_sum(True, xfwd.at[0], 0)
     joined(xr, 0, xfwd.at[0])
-    send_sum(xr, 0, True, xfin.at[0, 0], 2)
+    send_sum(xr, 0, True, sum_l.at[pl.ds(0, HALF)], 2)
     ph("j_near2b")
     wait_sum(False, xfwd.at[1], 0)
     joined(xl, 1, xfwd.at[1])
-    send_sum(xl, 1, False, xfin.at[1, 1], 2)
+    send_sum(xl, 1, False, sum_r.at[pl.ds(HALF, HALF)], 2)
 
     ph("d_own")
     group((x, x), (0, 1), 2, up=False)
@@ -592,17 +634,16 @@
         cp.wait()
 
     ph("fin_w1")
-    wait_sum(True, xfin.at[0, 1], 1)
-    wait_sum(False, xfin.at[1, 0], 1)
+    wait_sum(True, sum_l.at[pl.ds(HALF, HALF)], 1)
+    wait_sum(False, sum_r.at[pl.ds(0, HALF)], 1)
     ph("fin_w2")
-    wait_sum(True, xfin.at[0, 0], 2)
-    wait_sum(False, xfin.at[1, 1], 2)
+    wait_sum(True, sum_l.at[pl.ds(0, HALF)], 2)
+    wait_sum(False, sum_r.at[pl.ds(HALF, HALF)], 2)
 
     ph("drain")
     @pl.when(c != half)
     def _():
-        for cp in overs:
-            cp.wait_send()
+        over.wait_send()
 
     for cp in drains:
         cp.wait_send()
@@ -622,12 +663,12 @@
     any_ = pl.BlockSpec(memory_space=pl.ANY)
     vm = pl.BlockSpec(memory_space=pltpu.VMEM)
     dma = pltpu.SemaphoreType.DMA
-    part, sums = pl.pallas_call(
+    part, sum_l, sum_r = pl.pallas_call(
         kernel,
         out_shape=(jax.ShapeDtypeStruct((TOK, D), F32),
-                   jax.ShapeDtypeStruct((2, 2, HALF, D), BF16)),
+                   jax.ShapeDtypeStruct((TOK, D), BF16), jax.ShapeDtypeStruct((TOK, D), BF16)),
         in_specs=[any_, any_, any_, vm, any_, any_, vm, vm, any_],
-        out_specs=(any_, any_),
+        out_specs=(any_, any_, any_),
         scratch_shapes=[
             pltpu.VMEM((2, 4, 4, 128, CH), BF16),
             pltpu.VMEM((4, 4, 128, UG), BF16),
@@ -639,28 +680,27 @@
             pltpu.VMEM((TOK, D), BF16),
             pltpu.VMEM((TOK, D), BF16),
             pltpu.VMEM((8, 32, 256), BF16),
-            pltpu.VMEM((256, D), BF16),
             pltpu.VMEM((16, 8, HID), F32),
             pltpu.VMEM((4, TOK, HID), BF16),
             pltpu.VMEM((2, 4, 2, HALF, D), BF16),
             pltpu.VMEM((4, 2, HALF, D), BF16),
             pltpu.VMEM((2, HALF, D), BF16),
             pltpu.VMEM((TOK, D), F32),
-            dma((7,)), dma((2, 4)), dma((2, 4)),
+            dma((8,)), dma((4,)), dma((4,)),
             dma((4, 16)), dma((4, 16)),
-            dma((2, 16)), dma((2, 16)),
+            dma((16,)), dma((16,)),
             dma((2, 6)), dma((2, 6)),
-            dma((8,)), dma((8,)), dma((8,)), dma((8,)),
+            dma((8, 2)), dma((8, 2)), dma((8,)), dma((8,)),
             dma((8,)), dma((8,)),
             dma((4, 2)), dma((4, 2)),
             dma((2, 3)), dma((2, 3)),
+            dma((2, 2)), dma((2, 2)), dma((4,)), dma((4,)),
         ],
         compiler_params=pltpu.CompilerParams(
             collective_id=0, has_side_effects=True, vmem_limit_bytes=67_043_328),
     )(mixed, residual, mix_weight, norm_gain[None], up_weight.T, gate_weight.T, conv_weight, conv_bias,
       down_weight)
-    sums = sums.reshape(2, TOK, D).astype(F32)
-    return (part + sums[0] + sums[1]).astype(BF16)
+    return (part + sum_l.astype(F32) + sum_r.astype(F32)).astype(BF16)
 
 
 def solution(mesh):

time: 162 us -> 153 us (0.944)
  Pallas kernels: 157 us -> 148 us
  local copies, waits for them, and re-layouts: 2.87 us -> 0 us
  other arithmetic: 2.18 us -> 4.74 us
    pallas_call x1, Pallas kernels: 157 us -> 148 us  [body(): pl.pallas_call(kernel, out_shape=(jax.ShapeDtypeStruct((TOK, D), F32), ja...]
    slice x1 -> x0, local copies, waits for them, and re-layouts: 2.87 us -> none  [body(): return (part + sums[0] + sums[1]).astype(BF16)]
    convert_element_type x1, other arithmetic: 2.18 us -> 4.74 us  [body(): return (part + sum_l.astype(F32) + sum_r.astype(F32)).astype(BF16)]
where the time goes in v3:
time: 153 us; the launch traced here: 152 us
  Pallas kernels  148 us (97%)
  other arithmetic  4.74 us (3%)
    pallas_call x1, Pallas kernels, body(): pl.pallas_call(kernel, out_shape=(jax.ShapeDtypeStruct((TOK, D), F32), ja...  148 us
    convert_element_type x1, other arithmetic, body(): return (part + sum_l.astype(F32) + sum_r.astype(F32)).astype(BF16)  4.74 us

profile of v3, /device:TPU:1, one launch (start us, length us, event | category | flops | bytes accessed | tf_op | source)
XLA Modules:
  0.0 152.4 jit_solution(17688276046856939889)
XLA Ops:
  0.0 147.7 %shard_map.91 = (f32[384,2048]{1,0:T(8,128)}, bf16[384,2048]{1,0:T(8,128)(2,1)}, bf16[384,2048]{1,0:T(8,128)(2,1)}) custom-call(bf16[384,2048]{1,0:T(8,128)(2,1)} %mixed.1, bf16[384,2048]{1,0:T(8,128)(2,1)} %resid.1, bf16[16,2048]{1,0:T(8,128)(2,1)} %wm_in.1, f32[1,2048]{1,0:T(1,128)} %bitcast.5, bf16[688,128]{1,0:T(8,128)(2,1)} %bitcast.3, ...), custom_call_target="tpu_custom_call" | custom-call | tf_op jit(solution)/shard_map/pallas_call | solution.py:666
  147.7 4.7 %add_convert_fusion = bf16[384,2048]{1,0:T(8,128)(2,1)} fusion(bf16[384,2048]{1,0:T(8,128)(2,1)} %get-tuple-element.10, f32[384,2048]{1,0:T(8,128)} %get-tuple-element.8, bf16[384,2048]{1,0:T(8,128)(2,1)} %get-tuple-element.9), kind=kLoop, calls=%fused_computation | loop fusion | flops 3932160 | bytes 7864320 | tf_op jit(solution)/shard_map/convert_element_type | solution.py:703

commit v4 on v3

--- a/solution.py
+++ b/solution.py
@@ -40,7 +40,8 @@
 
 
 class Gather:
-    def __init__(self, ref, lo, rows, split, flip, fs, tp, send_sem, recv_sem):
+    def __init__(self, ref, lo, rows, split, flip, fs, tp, send_sem, recv_sem, total=None):
+        self.total = total
         self.ref, self.lo, self.rows, self.split, self.flip = ref, lo, rows, split, flip
         self.tp, self.ss, self.rs = tp, send_sem, recv_sem
         z, y = fs // 4, fs % 4
@@ -61,7 +62,7 @@
     def copy(self, k, blk, to):
         z, y = self.zy(*to)
         return pltpu.make_async_remote_copy(
-            src_ref=blk, dst_ref=blk, send_sem=self.ss.at[self.n % 16], recv_sem=self.rs.at[k],
+            src_ref=blk, dst_ref=blk, send_sem=self.ss if self.total is not None else self.ss.at[self.n], recv_sem=self.rs.at[k],
             device_id={"fs": z * 4 + y, "tp": self.tp}, device_id_type=MESH)
 
     def send(self, k, blk, to):
@@ -116,19 +117,23 @@
         self.wait(12 + i, self.view(self.REL[i], 2))
 
     def drain(self):
-        for c in self.sends:
-            c.wait_send()
-
-
-def kernel(mixed, resid, wm_in, gain, up_in, gate_in, cw_in, cb_in, dw_in, out, sum_l, sum_r,
+        if self.total is not None:
+            self.copy(0, self.total, (1, 0)).wait_send()
+        else:
+            for c in self.sends:
+                c.wait_send()
+
+
+def kernel(mixed, resid, wm_in, gain, up_in, gate_in, cw_in, cb_in, dw_in, out, last,
            wm, ug, dwn, upt, cw, tok, rr, mx, rs, hal, hu, hid, pbuf, precv, xfwd, base,
-           lsem, wx_s, wx_r, g_s, g_r, d_s, d_r, t_s, t_r, td_s, td_r, rd_s, rd_r, h_s, h_r,
-           p_s, p_r, x_s, x_r, xw_s, xw_r, xd_s, xd_r):
+           lsem, wx_s, wx_r, g_s, g_r, t_r, td_r, rd_r, p_r, x_r, xw_r, one):
     fs, tp = lax.axis_index("fs"), lax.axis_index("tp")
     z, y, x, c = fs // 4, fs % 4, tp // 2, tp % 2
     xr, xl, xo = (x + 1) % 4, (x + 3) % 4, (x + 2) % 4
     mate = x * 2 + (1 - c)
     drains = []
+    (w_sem, v_sem, d_s, d_r, t_s, td_s, rd_s, h_s, h_r, p_s, x_s, xw_s, xd_s, xd_r) = (
+        one.at[k] for k in range(14))
 
     def rcopy(src, dst, ss, rsem, tp_to, fs_to=None):
         return pltpu.make_async_remote_copy(
@@ -183,16 +188,17 @@
 
     lo = pl.multiple_of(c * 64, 64)
     other = pl.multiple_of(64 - lo, 64)
-    gw = Gather(wm.at[0], lo, 64, 32, c, fs, tp, g_s.at[0], g_r.at[0])
-    gv = Gather(wm.at[1], row16, 16, 16, c, fs, tp, g_s.at[1], g_r.at[1])
-    gu = Gather(ug, 0, 128, 64, c, fs, tp, g_s.at[2], g_r.at[2])
-    gd = Gather(dwn, 0, 688, 352, 1 - c, fs, tp, g_s.at[3], g_r.at[3])
+    gw = Gather(wm.at[0], lo, 64, 32, c, fs, tp, w_sem, g_r.at[0],
+                wm.at[0, pl.ds(0, 3), :, pl.ds(0, 80)])
+    gv = Gather(wm.at[1], row16, 16, 16, c, fs, tp, v_sem, g_r.at[1],
+                wm.at[1, pl.ds(0, 3), 0, pl.ds(0, 80)])
+    gu = Gather(ug, 0, 128, 64, c, fs, tp, g_s.at[0], g_r.at[2])
+    gd = Gather(dwn, 0, 688, 352, 1 - c, fs, tp, g_s.at[1], g_r.at[3])
 
     def share(k, dp, ds):
         blk = gw.view(dp, ds)
-        cp = rcopy(blk, blk, d_s.at[k], d_r.at[k], mate)
-        cp.start()
-        drains.append(cp)
+        cp = rcopy(blk, blk, d_s, d_r, mate)
+        cp.start()
 
     def w_cross(i):
         gw.cross(i)
@@ -204,19 +210,17 @@
 
     def line_send(to_right, k, xsrc, z0, nz):
         side, blk = 0 if to_right else 1, w_rows(xsrc, c, z0, nz)
-        cp = rcopy(blk, blk, xw_s.at[side, k], xw_r.at[side, k], (xr if to_right else xl) * 2 + c)
-        cp.start()
-        drains.append(cp)
+        cp = rcopy(blk, blk, xw_s, xw_r.at[side, k], (xr if to_right else xl) * 2 + c)
+        cp.start()
 
     def line_wait(from_left, k, xsrc, z0, nz):
         side, blk = 0 if from_left else 1, w_rows(xsrc, c, z0, nz)
-        rcopy(blk, blk, xw_s.at[side, k], xw_r.at[side, k], mate).wait_recv()
-
-    def line_share(k, xsrc):
+        rcopy(blk, blk, xw_s, xw_r.at[side, k], mate).wait_recv()
+
+    def line_share(xsrc):
         blk = w_rows(xsrc, c)
-        cp = rcopy(blk, blk, xd_s.at[k], xd_r.at[k], mate)
-        cp.start()
-        drains.append(cp)
+        cp = rcopy(blk, blk, xd_s, xd_r, mate)
+        cp.start()
 
     ph("v_start")
     ld_own.wait()
@@ -265,15 +269,14 @@
     def send_tok(xsrc, h, ch, to_right, sidx):
         blk = tok.at[xsrc, c, ch, pl.ds(h * HALF, HALF)]
         side = 0 if to_right else 1
-        cp = rcopy(blk, blk, t_s.at[side, sidx], t_r.at[side, sidx],
+        cp = rcopy(blk, blk, t_s, t_r.at[side, sidx],
                    (xr if to_right else xl) * 2 + c)
         cp.start()
-        drains.append(cp)
 
     def tok_wait(from_left, idx, xsrc, h, ch):
         blk = tok.at[xsrc, c, ch, pl.ds(h * HALF, HALF)]
         side = 0 if from_left else 1
-        rcopy(blk, blk, t_s.at[side, idx], t_r.at[side, idx], mate).wait_recv()
+        rcopy(blk, blk, t_s, t_r.at[side, idx], mate).wait_recv()
 
     def factor(xsrc, h):
         acc = None
@@ -286,23 +289,20 @@
 
     def pass_on(k, xsrc, h, ch):
         blk = tok.at[xsrc, c, ch, pl.ds(h * HALF, HALF)]
-        cp = rcopy(blk, blk, td_s.at[k, ch], td_r.at[k, ch], mate)
-        cp.start()
-        drains.append(cp)
+        cp = rcopy(blk, blk, td_s, td_r.at[k], mate)
+        cp.start()
 
     def pass_factor(k, xsrc, h):
         factor(xsrc, h)
         blk = rr.at[xsrc, c, h]
-        cp = rcopy(blk, blk, rd_s.at[k], rd_r.at[k], mate)
-        cp.start()
-        drains.append(cp)
+        cp = rcopy(blk, blk, rd_s, rd_r.at[k], mate)
+        cp.start()
 
     def mate_wait(k, xsrc, h):
-        for ch in range(2):
-            blk = tok.at[xsrc, 1 - c, ch, pl.ds(h * HALF, HALF)]
-            rcopy(blk, blk, td_s.at[k, ch], td_r.at[k, ch], mate).wait_recv()
+        blk = tok.at[xsrc, 1 - c, :, pl.ds(h * HALF, HALF)]
+        rcopy(blk, blk, td_s, td_r.at[k], mate).wait_recv()
         blk = rr.at[xsrc, 1 - c, h]
-        rcopy(blk, blk, rd_s.at[k], rd_r.at[k], mate).wait_recv()
+        rcopy(blk, blk, rd_s, rd_r.at[k], mate).wait_recv()
 
     ph("w_near")
     gw.near()
@@ -319,7 +319,7 @@
         gv.last(i)
     line_send(True, 0, x, 0, 4)
     line_send(False, 0, x, 0, 4)
-    line_share(0, x)
+    line_share(x)
     ph("w_far")
     gw.far()
     share(3, 2, 0)
@@ -337,14 +337,13 @@
     ph("line_fwd")
     line_wait(True, 0, xl, 0, 4)
     line_send(True, 1, xl, 0, 2)
-    line_share(1, xl)
+    line_share(xl)
     line_wait(False, 0, xr, 0, 4)
     line_send(False, 1, xr, 2, 2)
-    line_share(2, xr)
+    line_share(xr)
     ph("w_shared")
-    for k in range(16):
-        blk = wm.at[0, k // 4, k % 4, pl.ds(other, 64)]
-        rcopy(blk, blk, d_s.at[k], d_r.at[k], mate).wait_recv()
+    blk = wm.at[0, :, :, pl.ds(other, 64)]
+    rcopy(blk, blk, d_s, d_r, mate).wait_recv()
     ld_mx.wait()
     ld_rs.wait()
     ph("mix0")
@@ -359,10 +358,9 @@
     ph("line_far")
     line_wait(True, 1, xo, 0, 2)
     line_wait(False, 1, xo, 2, 2)
-    line_share(3, xo)
-    for k, xsrc in enumerate((x, xl, xr, xo)):
-        blk = w_rows(xsrc, 1 - c)
-        rcopy(blk, blk, xd_s.at[k], xd_r.at[k], mate).wait_recv()
+    line_share(xo)
+    blk = wm.at[1, :, :, pl.ds(0, 64)]
+    rcopy(blk, blk, xd_s, xd_r, mate).wait_recv()
     ph("mix1")
     mix(1, 0)
     mix(1, 1)
@@ -386,9 +384,7 @@
                 tails.append(v[r + 8:r + 9] * f[r:r + 1])
     hal[tp] = jnp.concatenate(tails, axis=0).astype(BF16)
     for k in range(1, 8):
-        cp = rcopy(hal.at[tp], hal.at[tp], h_s.at[k], h_r.at[8 - k], (tp + k) % 8)
-        cp.start()
-        drains.append(cp)
+        rcopy(hal.at[tp], hal.at[tp], h_s, h_r, (tp + k) % 8).start()
 
     ph("gu_far")
     gu.far()
@@ -427,9 +423,8 @@
     gd.near()
 
     ph("xexp")
-    for k in range(1, 8):
-        src = (tp + k) % 8
-        rcopy(hal.at[src], hal.at[src], h_s.at[k], h_r.at[k], mate).wait_recv()
+    blk = hal.at[pl.ds(0, 7)]
+    rcopy(blk, blk, h_s, h_r, mate).wait_recv()
     hv = hal[...].reshape(256, 256).astype(F32)
     rid = lax.broadcasted_iota(jnp.int32, (256, 256), 0) % 8
     for q in range(8):
@@ -494,7 +489,7 @@
         @pl.when(cls == 0)
         def _():
             for k in range(2):
-                rcopy(pbuf.at[0, xs[k], hs[k]], precv.at[xs[k], hs[k]], p_s.at[xs[k], hs[k]],
+                rcopy(pbuf.at[0, xs[k], hs[k]], precv.at[xs[k], hs[k]], p_s,
                       p_r.at[xs[k], hs[k]], mate).start()
 
     def core_of(cls):
@@ -510,7 +505,7 @@
                 down(to, xs, hs, cls)
 
     def joined(xx, h, extra=None):
-        rcopy(pbuf.at[0, xx, h], precv.at[xx, h], p_s.at[xx, h], p_r.at[xx, h], mate).wait_recv()
+        rcopy(pbuf.at[0, xx, h], precv.at[xx, h], p_s, p_r.at[xx, h], mate).wait_recv()
 
         @pl.loop(0, HALF // 16)
         def _(r):
@@ -522,14 +517,13 @@
 
     def send_sum(xx, h, to_right, dst, k):
         side = 0 if to_right else 1
-        cp = rcopy(pbuf.at[1, xx, h], dst, x_s.at[side, k], x_r.at[side, k],
+        cp = rcopy(pbuf.at[1, xx, h], dst, x_s, x_r.at[side, k],
                    (xr if to_right else xl) * 2 + c)
         cp.start()
-        drains.append(cp)
 
     def wait_sum(from_left, dst, k):
         side = 0 if from_left else 1
-        rcopy(dst, dst, x_s.at[side, k], x_r.at[side, k], mate).wait_recv()
+        rcopy(dst, dst, x_s, x_r.at[side, k], mate).wait_recv()
 
     ph("gd_far")
     gd.far()
@@ -582,9 +576,9 @@
     group((xr, xl), (1, 0))
     ph("j_near1")
     joined(xr, 1)
-    send_sum(xr, 1, True, sum_l.at[pl.ds(HALF, HALF)], 1)
+    send_sum(xr, 1, True, rs.at[pl.ds(HALF, HALF)], 1)
     joined(xl, 0)
-    send_sum(xl, 0, False, sum_r.at[pl.ds(0, HALF)], 1)
+    send_sum(xl, 0, False, rs.at[pl.ds(0, HALF)], 1)
 
     ph("tok_near2")
     tok_wait(True, 4, xl, 1, 0)
@@ -604,18 +598,18 @@
     ph("j_near2")
     wait_sum(True, xfwd.at[0], 0)
     joined(xr, 0, xfwd.at[0])
-    send_sum(xr, 0, True, sum_l.at[pl.ds(0, HALF)], 2)
+    send_sum(xr, 0, True, last.at[pl.ds(0, HALF)], 2)
     ph("j_near2b")
     wait_sum(False, xfwd.at[1], 0)
     joined(xl, 1, xfwd.at[1])
-    send_sum(xl, 1, False, sum_r.at[pl.ds(HALF, HALF)], 2)
+    send_sum(xl, 1, False, last.at[pl.ds(HALF, HALF)], 2)
 
     ph("d_own")
     group((x, x), (0, 1), 2, up=False)
     ph("base")
     outs = []
     for h in range(2):
-        rcopy(pbuf.at[0, x, h], precv.at[x, h], p_s.at[x, h], p_r.at[x, h], mate).wait_recv()
+        rcopy(pbuf.at[0, x, h], precv.at[x, h], p_s, p_r.at[x, h], mate).wait_recv()
 
         @pl.loop(0, HALF // 16)
         def _(r):
@@ -626,6 +620,15 @@
                 v = tok[x, c, ch, at, :].astype(F32) + pbuf[1, x, h, row, cols].astype(F32)
                 base[at, cols] = v + precv[x, h, row, cols].astype(F32)
 
+    ph("fin_w1")
+    wait_sum(True, rs.at[pl.ds(HALF, HALF)], 1)
+    wait_sum(False, rs.at[pl.ds(0, HALF)], 1)
+    for h in range(2):
+        @pl.loop(h * 12, h * 12 + 12)
+        def _(r):
+            at = pl.ds(pl.multiple_of(r * 16, 16), 16)
+            base[at, :] = base[at, :] + rs[at, :].astype(F32)
+
         cp = pltpu.make_async_copy(base.at[pl.ds(h * HALF, HALF)], out.at[pl.ds(h * HALF, HALF)],
                                    lsem.at[5 + h])
         cp.start()
@@ -633,12 +636,9 @@
     for cp in outs:
         cp.wait()
 
-    ph("fin_w1")
-    wait_sum(True, sum_l.at[pl.ds(HALF, HALF)], 1)
-    wait_sum(False, sum_r.at[pl.ds(0, HALF)], 1)
     ph("fin_w2")
-    wait_sum(True, sum_l.at[pl.ds(0, HALF)], 2)
-    wait_sum(False, sum_r.at[pl.ds(HALF, HALF)], 2)
+    wait_sum(True, last.at[pl.ds(0, HALF)], 2)
+    wait_sum(False, last.at[pl.ds(HALF, HALF)], 2)
 
     ph("drain")
     @pl.when(c != half)
@@ -651,10 +651,17 @@
     gv.drain()
     gu.drain()
     gd.drain()
-    for xx in range(4):
-        for h in range(2):
-            rcopy(pbuf.at[0, xx, h], precv.at[xx, h], p_s.at[xx, h], p_r.at[xx, h],
-                  mate).wait_send()
+    for sem, view in (
+            (d_s, wm.at[0, :, :, pl.ds(0, 64)]),
+            (xw_s, wm.at[1, :, :, pl.ds(0, 48)]),
+            (xd_s, wm.at[1, :, :, pl.ds(0, 64)]),
+            (t_s, tok.at[pl.ds(0, 3), 0]),
+            (td_s, tok.at[:, 0]),
+            (rd_s, rr.at[:, 0]),
+            (h_s, hal.at[pl.ds(0, 7)]),
+            (p_s, pbuf.at[0]),
+            (x_s, precv.at[pl.ds(0, 3)])):
+        rcopy(view, view, sem, lsem.at[0], mate).wait_send()
     ph("")
 
 
@@ -663,12 +670,12 @@
     any_ = pl.BlockSpec(memory_space=pl.ANY)
     vm = pl.BlockSpec(memory_space=pltpu.VMEM)
     dma = pltpu.SemaphoreType.DMA
-    part, sum_l, sum_r = pl.pallas_call(
+    part, last = pl.pallas_call(
         kernel,
         out_shape=(jax.ShapeDtypeStruct((TOK, D), F32),
-                   jax.ShapeDtypeStruct((TOK, D), BF16), jax.ShapeDtypeStruct((TOK, D), BF16)),
+                   jax.ShapeDtypeStruct((TOK, D), BF16)),
         in_specs=[any_, any_, any_, vm, any_, any_, vm, vm, any_],
-        out_specs=(any_, any_, any_),
+        out_specs=(any_, any_),
         scratch_shapes=[
             pltpu.VMEM((2, 4, 4, 128, CH), BF16),
             pltpu.VMEM((4, 4, 128, UG), BF16),
@@ -687,20 +694,16 @@
             pltpu.VMEM((2, HALF, D), BF16),
             pltpu.VMEM((TOK, D), F32),
             dma((8,)), dma((4,)), dma((4,)),
-            dma((4, 16)), dma((4, 16)),
-            dma((16,)), dma((16,)),
-            dma((2, 6)), dma((2, 6)),
-            dma((8, 2)), dma((8, 2)), dma((8,)), dma((8,)),
-            dma((8,)), dma((8,)),
-            dma((4, 2)), dma((4, 2)),
-            dma((2, 3)), dma((2, 3)),
-            dma((2, 2)), dma((2, 2)), dma((4,)), dma((4,)),
+            dma((2, 16)), dma((4, 16)),
+            dma((2, 6)), dma((8,)), dma((8,)),
+            dma((4, 2)), dma((2, 3)), dma((2, 2)),
+            dma((14,)),
         ],
         compiler_params=pltpu.CompilerParams(
             collective_id=0, has_side_effects=True, vmem_limit_bytes=67_043_328),
     )(mixed, residual, mix_weight, norm_gain[None], up_weight.T, gate_weight.T, conv_weight, conv_bias,
       down_weight)
-    return (part + sum_l.astype(F32) + sum_r.astype(F32)).astype(BF16)
+    return (part + last.astype(F32)).astype(BF16)
 
 
 def solution(mesh):

time: 153 us -> 151 us (0.987)
  Pallas kernels: 148 us -> 146 us
where the time goes in v4:
time: 151 us; the launch traced here: 150 us
  Pallas kernels  146 us (97%)
  other arithmetic  4.01 us (3%)
    pallas_call x1, Pallas kernels, body(): pl.pallas_call(kernel, out_shape=(jax.ShapeDtypeStruct((TOK, D), F32), ja...  146 us
    convert_element_type x1, other arithmetic, body(): return (part + last.astype(F32)).astype(BF16)  4.01 us

profile of v4, /device:TPU:1, one launch (start us, length us, event | category | flops | bytes accessed | tf_op | source)
XLA Modules:
  0.0 150.3 jit_solution(11859950299920120525)
XLA Ops:
  0.0 146.3 %shard_map.91 = (f32[384,2048]{1,0:T(8,128)}, bf16[384,2048]{1,0:T(8,128)(2,1)}) custom-call(bf16[384,2048]{1,0:T(8,128)(2,1)} %mixed.1, bf16[384,2048]{1,0:T(8,128)(2,1)} %resid.1, bf16[16,2048]{1,0:T(8,128)(2,1)} %wm_in.1, f32[1,2048]{1,0:T(1,128)} %bitcast.5, bf16[688,128]{1,0:T(8,128)(2,1)} %bitcast.3, bf16[688,128]{1,0:T(8,128)(2,1)} %bitcast.4, ...), custom_call_target="tpu_custom_call" | custom-call | tf_op jit(solution)/shard_map/pallas_call | solution.py:673
  146.3 4.0 %add_convert_fusion = bf16[384,2048]{1,0:T(8,128)(2,1)} fusion(f32[384,2048]{1,0:T(8,128)} %get-tuple-element.7, bf16[384,2048]{1,0:T(8,128)(2,1)} %get-tuple-element.8), kind=kLoop, calls=%fused_computation | loop fusion | flops 2359296 | bytes 6291456 | tf_op jit(solution)/shard_map/convert_element_type | solution.py:706

commit v5 on v4

--- a/solution.py
+++ b/solution.py
@@ -217,8 +217,8 @@
         side, blk = 0 if from_left else 1, w_rows(xsrc, c, z0, nz)
         rcopy(blk, blk, xw_s, xw_r.at[side, k], mate).wait_recv()
 
-    def line_share(xsrc):
-        blk = w_rows(xsrc, c)
+    def line_share(xsrc, z0=0, nz=4):
+        blk = w_rows(xsrc, c, z0, nz)
         cp = rcopy(blk, blk, xd_s, xd_r, mate)
         cp.start()
 
@@ -317,8 +317,10 @@
     gv.cross(3)
     for i in range(4):
         gv.last(i)
-    line_send(True, 0, x, 0, 4)
-    line_send(False, 0, x, 0, 4)
+    line_send(True, 0, x, 0, 2)
+    line_send(False, 0, x, 2, 2)
+    line_send(True, 2, x, 2, 2)
+    line_send(False, 2, x, 0, 2)
     line_share(x)
     ph("w_far")
     gw.far()
@@ -335,12 +337,12 @@
         gw.last(i)
         share(12 + i, Gather.REL[i], 2)
     ph("line_fwd")
-    line_wait(True, 0, xl, 0, 4)
+    line_wait(True, 0, xl, 0, 2)
     line_send(True, 1, xl, 0, 2)
-    line_share(xl)
-    line_wait(False, 0, xr, 0, 4)
+    line_share(xl, 0, 2)
+    line_wait(False, 0, xr, 2, 2)
     line_send(False, 1, xr, 2, 2)
-    line_share(xr)
+    line_share(xr, 2, 2)
     ph("w_shared")
     blk = wm.at[0, :, :, pl.ds(other, 64)]
     rcopy(blk, blk, d_s, d_r, mate).wait_recv()
@@ -356,6 +358,10 @@
     ph("gu_near")
     gu.near()
     ph("line_far")
+    line_wait(True, 2, xl, 2, 2)
+    line_share(xl, 2, 2)
+    line_wait(False, 2, xr, 0, 2)
+    line_share(xr, 0, 2)
     line_wait(True, 1, xo, 0, 2)
     line_wait(False, 1, xo, 2, 2)
     line_share(xo)
@@ -527,17 +533,9 @@
 
     ph("gd_far")
     gd.far()
-    ph("mate_own")
-    mate_wait(0, x, 0)
-    mate_wait(1, x, 1)
-    ph("h_own0")
-    hidden((x, x), (0, 1), core_of(0), 2)
-    ph("gd_c12")
+    ph("gd_c123")
     gd.cross(1)
     gd.cross(2)
-    ph("h_own1")
-    hidden((x, x), (0, 1), core_of(1), 3)
-    ph("gd_c3")
     gd.cross(3)
 
     ph("tok_opp")
@@ -604,8 +602,11 @@
     joined(xl, 1, xfwd.at[1])
     send_sum(xl, 1, False, last.at[pl.ds(HALF, HALF)], 2)
 
-    ph("d_own")
-    group((x, x), (0, 1), 2, up=False)
+    ph("mate_own")
+    mate_wait(0, x, 0)
+    mate_wait(1, x, 1)
+    ph("g_own")
+    group((x, x), (0, 1))
     ph("base")
     outs = []
     for h in range(2):
@@ -688,7 +689,7 @@
             pltpu.VMEM((TOK, D), BF16),
             pltpu.VMEM((8, 32, 256), BF16),
             pltpu.VMEM((16, 8, HID), F32),
-            pltpu.VMEM((4, TOK, HID), BF16),
+            pltpu.VMEM((2, TOK, HID), BF16),
             pltpu.VMEM((2, 4, 2, HALF, D), BF16),
             pltpu.VMEM((4, 2, HALF, D), BF16),
             pltpu.VMEM((2, HALF, D), BF16),
@@ -696,7 +697,7 @@
             dma((8,)), dma((4,)), dma((4,)),
             dma((2, 16)), dma((4, 16)),
             dma((2, 6)), dma((8,)), dma((8,)),
-            dma((4, 2)), dma((2, 3)), dma((2, 2)),
+            dma((4, 2)), dma((2, 3)), dma((2, 3)),
             dma((14,)),
         ],
         compiler_params=pltpu.CompilerParams(

time: 151 us -> 150 us (level)
  no operation moved by 1% of the time
where the time goes in v5:
time: 150 us
  Pallas kernels  146 us (97%)
  other arithmetic  4.01 us (3%)
    pallas_call x1, Pallas kernels, body(): pl.pallas_call(kernel, out_shape=(jax.ShapeDtypeStruct((TOK, D), F32), ja...  146 us
    convert_element_type x1, other arithmetic, body(): return (part + last.astype(F32)).astype(BF16)  4.01 us

profile of v5, /device:TPU:1, one launch (start us, length us, event | category | flops | bytes accessed | tf_op | source)
XLA Modules:
  0.0 149.5 jit_solution(18083071261760013123)
XLA Ops:
  0.0 145.5 %shard_map.91 = (f32[384,2048]{1,0:T(8,128)}, bf16[384,2048]{1,0:T(8,128)(2,1)}) custom-call(bf16[384,2048]{1,0:T(8,128)(2,1)} %mixed.1, bf16[384,2048]{1,0:T(8,128)(2,1)} %resid.1, bf16[16,2048]{1,0:T(8,128)(2,1)} %wm_in.1, f32[1,2048]{1,0:T(1,128)} %bitcast.5, bf16[688,128]{1,0:T(8,128)(2,1)} %bitcast.3, bf16[688,128]{1,0:T(8,128)(2,1)} %bitcast.4, ...), custom_call_target="tpu_custom_call" | custom-call | tf_op jit(solution)/shard_map/pallas_call | solution.py:674
  145.5 4.0 %add_convert_fusion = bf16[384,2048]{1,0:T(8,128)(2,1)} fusion(f32[384,2048]{1,0:T(8,128)} %get-tuple-element.7, bf16[384,2048]{1,0:T(8,128)(2,1)} %get-tuple-element.8), kind=kLoop, calls=%fused_computation | loop fusion | flops 2359296 | bytes 6291456 | tf_op jit(solution)/shard_map/convert_element_type | solution.py:707

commit v6 on v5

--- a/solution.py
+++ b/solution.py
@@ -40,7 +40,9 @@
 
 
 class Gather:
-    def __init__(self, ref, lo, rows, split, flip, fs, tp, send_sem, recv_sem, total=None):
+    def __init__(self, ref, lo, rows, split, flip, fs, tp, send_sem, recv_sem, total=None,
+                 direct=False):
+        self.direct = direct
         self.total = total
         self.ref, self.lo, self.rows, self.split, self.flip = ref, lo, rows, split, flip
         self.tp, self.ss, self.rs = tp, send_sem, recv_sem
@@ -80,17 +82,22 @@
         blk = self.view(self.REL[i], 0)
         self.send(4 + i, blk, (0, 1))
         self.send(8 + i, blk, (0, -1))
+        if self.direct:
+            self.send(12 + i, blk, (0, 2))
 
     def start(self):
         own = self.view(0, 0)
         self.send(0, own, (1, 0))
         self.send(1, own, (-1, 0))
+        if self.direct:
+            self.send(2, own, (2, 0))
         self.both(0)
 
     def near(self):
         s = self.split
         self.wait(0, self.view(-1, 0))
-        self.send(2, self.view(-1, 0, 0, s), (1, 0))
+        if not self.direct:
+            self.send(2, self.view(-1, 0, 0, s), (1, 0))
         self.both(1)
         self.wait(1, self.view(1, 0))
         if s < self.rows:
@@ -107,10 +114,10 @@
     def cross(self, i):
         below, above = self.view(self.REL[i], -1), self.view(self.REL[i], 1)
         self.wait(4 + i, below)
-        if i < 2:
+        if i < 2 and not self.direct:
             self.send(12 + i, below, (0, 1))
         self.wait(8 + i, above)
-        if i >= 2:
+        if i >= 2 and not self.direct:
             self.send(12 + i, above, (0, -1))
 
     def last(self, i):
@@ -162,6 +169,7 @@
     peers = [(fs, (tp + k) % 8) for k in range(1, 8)]
     peers += [(z * 4 + (y + 1) % 4, tp), (z * 4 + (y + 3) % 4, tp)]
     peers += [(((z + 1) % 4) * 4 + y, tp), (((z + 3) % 4) * 4 + y, tp)]
+    peers += [(z * 4 + (y + 2) % 4, tp), (((z + 2) % 4) * 4 + y, tp)]
     for f, t in peers:
         pl.semaphore_signal(bar, inc=1, device_id={"fs": f, "tp": t}, device_id_type=MESH)
     pl.semaphore_wait(bar, len(peers))
@@ -191,7 +199,7 @@
     gw = Gather(wm.at[0], lo, 64, 32, c, fs, tp, w_sem, g_r.at[0],
                 wm.at[0, pl.ds(0, 3), :, pl.ds(0, 80)])
     gv = Gather(wm.at[1], row16, 16, 16, c, fs, tp, v_sem, g_r.at[1],
-                wm.at[1, pl.ds(0, 3), 0, pl.ds(0, 80)])
+                wm.at[1, pl.ds(0, 3), 0, pl.ds(0, 80)], True)
     gu = Gather(ug, 0, 128, 64, c, fs, tp, g_s.at[0], g_r.at[2])
     gd = Gather(dwn, 0, 688, 352, 1 - c, fs, tp, g_s.at[1], g_r.at[3])
 
@@ -226,6 +234,7 @@
     ld_own.wait()
     gv.start()
     gv.near()
+    gv.far()
     ph("w_start")
     for k in range(4):
         row = pl.multiple_of(lo + k * 16, 16)
@@ -233,10 +242,6 @@
         rcopy(blk, blk, wx_s.at[0], wx_r.at[k], mate).wait_recv()
     gw.start()
     share(0, 0, 0)
-    ph("v_far")
-    gv.cross(0)
-    gv.far()
-
     ph("prep")
     zero_rows = jnp.zeros((HID - 688, 128), BF16)
 
@@ -308,14 +313,11 @@
     gw.near()
     share(1, -1, 0)
     share(2, 1, 0)
-    ph("v_c12")
-    gv.cross(1)
-    gv.cross(2)
     ph("w_c0")
     w_cross(0)
     ph("v_last")
-    gv.cross(3)
     for i in range(4):
+        gv.cross(i)
         gv.last(i)
     line_send(True, 0, x, 0, 2)
     line_send(False, 0, x, 2, 2)

time: 150 us -> 147 us (0.980)
  Pallas kernels: 146 us -> 143 us
    pallas_call x1, Pallas kernels: 146 us -> 143 us  [body(): pl.pallas_call(kernel, out_shape=(jax.ShapeDtypeStruct((TOK, D), F32), ja...]
where the time goes in v6:
time: 147 us
  Pallas kernels  143 us (97%)
  other arithmetic  4.01 us (3%)
    pallas_call x1, Pallas kernels, body(): pl.pallas_call(kernel, out_shape=(jax.ShapeDtypeStruct((TOK, D), F32), ja...  143 us
    convert_element_type x1, other arithmetic, body(): return (part + last.astype(F32)).astype(BF16)  4.01 us

profile of v6, /device:TPU:1, one launch (start us, length us, event | category | flops | bytes accessed | tf_op | source)
XLA Modules:
  0.0 146.7 jit_solution(336374748374674077)
XLA Ops:
  0.0 142.7 %shard_map.91 = (f32[384,2048]{1,0:T(8,128)}, bf16[384,2048]{1,0:T(8,128)(2,1)}) custom-call(bf16[384,2048]{1,0:T(8,128)(2,1)} %mixed.1, bf16[384,2048]{1,0:T(8,128)(2,1)} %resid.1, bf16[16,2048]{1,0:T(8,128)(2,1)} %wm_in.1, f32[1,2048]{1,0:T(1,128)} %bitcast.5, bf16[688,128]{1,0:T(8,128)(2,1)} %bitcast.3, bf16[688,128]{1,0:T(8,128)(2,1)} %bitcast.4, ...), custom_call_target="tpu_custom_call" | custom-call | tf_op jit(solution)/shard_map/pallas_call | solution.py:676
  142.7 4.0 %add_convert_fusion = bf16[384,2048]{1,0:T(8,128)(2,1)} fusion(f32[384,2048]{1,0:T(8,128)} %get-tuple-element.7, bf16[384,2048]{1,0:T(8,128)(2,1)} %get-tuple-element.8), kind=kLoop, calls=%fused_computation | loop fusion | flops 2359296 | bytes 6291456 | tf_op jit(solution)/shard_map/convert_element_type | solution.py:709

commit v7 on v6

--- a/solution.py
+++ b/solution.py
@@ -334,10 +334,6 @@
     ph("w_c3")
     w_cross(3)
     gu.start()
-    ph("w_last")
-    for i in range(4):
-        gw.last(i)
-        share(12 + i, Gather.REL[i], 2)
     ph("line_fwd")
     line_wait(True, 0, xl, 0, 2)
     line_send(True, 1, xl, 0, 2)
@@ -345,6 +341,10 @@
     line_wait(False, 0, xr, 2, 2)
     line_send(False, 1, xr, 2, 2)
     line_share(xr, 2, 2)
+    ph("w_last")
+    for i in range(4):
+        gw.last(i)
+        share(12 + i, Gather.REL[i], 2)
     ph("w_shared")
     blk = wm.at[0, :, :, pl.ds(other, 64)]
     rcopy(blk, blk, d_s, d_r, mate).wait_recv()

time: 147 us -> 146 us (level)
  no operation moved by 1% of the time
where the time goes in v7:
time: 146 us
  Pallas kernels  142 us (97%)
  other arithmetic  4.01 us (3%)
    pallas_call x1, Pallas kernels, body(): pl.pallas_call(kernel, out_shape=(jax.ShapeDtypeStruct((TOK, D), F32), ja...  142 us
    convert_element_type x1, other arithmetic, body(): return (part + last.astype(F32)).astype(BF16)  4.01 us

profile of v7, /device:TPU:1, one launch (start us, length us, event | category | flops | bytes accessed | tf_op | source)
XLA Modules:
  0.0 146.1 jit_solution(5882963497061741041)
XLA Ops:
  0.0 142.0 %shard_map.91 = (f32[384,2048]{1,0:T(8,128)}, bf16[384,2048]{1,0:T(8,128)(2,1)}) custom-call(bf16[384,2048]{1,0:T(8,128)(2,1)} %mixed.1, bf16[384,2048]{1,0:T(8,128)(2,1)} %resid.1, bf16[16,2048]{1,0:T(8,128)(2,1)} %wm_in.1, f32[1,2048]{1,0:T(1,128)} %bitcast.5, bf16[688,128]{1,0:T(8,128)(2,1)} %bitcast.3, bf16[688,128]{1,0:T(8,128)(2,1)} %bitcast.4, ...), custom_call_target="tpu_custom_call" | custom-call | tf_op jit(solution)/shard_map/pallas_call | solution.py:676
  142.0 4.0 %add_convert_fusion = bf16[384,2048]{1,0:T(8,128)(2,1)} fusion(f32[384,2048]{1,0:T(8,128)} %get-tuple-element.7, bf16[384,2048]{1,0:T(8,128)(2,1)} %get-tuple-element.8), kind=kLoop, calls=%fused_computation | loop fusion | flops 2359296 | bytes 6291456 | tf_op jit(solution)/shard_map/convert_element_type | solution.py:709
